TPU v7x, 32 devices: a whole 2x2x4 slice. The times are simulated.
32 devices in a mesh: sp: 8 (over z, x), tp: 4 (over y, core).
Axes of the slice: x: 2, y: 2, z: 4, core: 2. Of those that a mesh axis runs over, the one named last changes fastest.
Arguments:
- incoming_residual_stream: bfloat16 [4096, 2048], P(('sp', 'tp')), may hold values from -6 to 6
- result_valve: bfloat16 [4096, 2048], P('sp', 'tp'), may hold values from -6 to 6
- channel_feed_matrix: bfloat16 [4096, 2048], P('sp', 'tp'), may hold values from -6 to 6
- memory_feed_matrix: bfloat16 [4096, 512], P('sp', 'tp'), may hold values from -6 to 6
- memory_query_matrix: bfloat16 [4096, 512], P('sp', 'tp'), may hold values from -6 to 6
- unsoftened_deltas: float32 [4096, 32], P('sp', 'tp'), may hold values from -2.7 to 2.7
- delta_offset: float32 [32], P('tp'), may hold values from -4.5 to -3.5
- channel_fading_speed: float32 [32], P('tp'), as said below
- extra_log_fading: float32 [4096, 32], P('sp', 'tp'), may hold values from -0.7 to 0
- bypass_factor: float32 [32], P('tp'), may hold values from 0.1 to 1.9
- channel_feed_kernel: bfloat16 [4, 2048], P(None, 'tp'), may hold values from -3 to 3
- memory_feed_kernel: bfloat16 [4, 512], P(None, 'tp'), may hold values from -3 to 3
- memory_query_kernel: bfloat16 [4, 512], P(None, 'tp'), may hold values from -3 to 3
- cluster_scaling_vector: float32 [2048], P('tp'), may hold values from 0.1 to 1.9
- mixer_result_matrix: bfloat16 [2048, 2048], P('tp'), may hold values from -0.125 to 0.125
- initial_scaling_vector: float32 [2048], replicated, may hold values from 0.1 to 1.9
- valve_matrix: bfloat16 [2048, 5632], P('sp', 'tp'), may hold values from -0.125 to 0.125
- widen_matrix: bfloat16 [2048, 5632], P('sp', 'tp'), may hold values from -0.125 to 0.125
- shrink_matrix: bfloat16 [5632, 2048], P('tp', 'sp'), may hold values from -0.078125 to 0.078125
- valve_filter_kernel: bfloat16 [3, 5632], P(None, 'tp'), may hold values from -3.5 to 3.5
- widen_filter_kernel: bfloat16 [3, 5632], P(None, 'tp'), may hold values from -3.5 to 3.5
- latter_scaling_vector: float32 [2048], replicated, may hold values from 0.1 to 1.9
Outputs:
- layer_out: bfloat16 [4096, 2048], P(('sp', 'tp'))
Inputs may be any that keep to these rules, and one draw needn't show every extreme that they name: `channel_fading_speed`: positive.
All inputs are finite; a program needn't handle non-finite values.
Results may differ from a plain program's by a relative error of at most 0.02.
Values may be sent and summed in bfloat16 or wider, within the bound.
A program may use at most 128 MiB of HBM per device.

v0:
```python
import functools
import jax
import jax.numpy as jnp
from jax import lax
from jax.experimental import pallas as pl
from jax.experimental.pallas import tpu as pltpu
from jax.sharding import PartitionSpec as P

HEADS = 32
HEAD_DIM = 64
GROUPS = 4
STATE = 128
CONV = 4
FCONV = 3
BLOCK = 128


EPSILON = 1e-05
ALPHA = 2.0**0.25
HIGHEST = lax.Precision.HIGHEST


def shifted(shard, axis, by):
    count = lax.axis_size(axis)
    pairs = [(i, i + by) for i in range(count) if 0 <= i + by < count]
    return lax.ppermute(shard, axis, pairs)


def entering(shard, axis, join, neutral):
    place = lax.axis_index(axis)
    gathered = jax.tree.map(
        lambda a, kind: lax.all_gather(a.astype(kind), axis), shard, (jnp.bfloat16, jnp.bfloat16)
    )
    state = jax.tree.map(lambda a, e: jnp.zeros_like(a) + jnp.asarray(e, a.dtype), shard, neutral)

    def one(lap, state):
        return join(
            state,
            jax.tree.map(
                lambda a, own: lax.dynamic_index_in_dim(a, lap, 0, False).astype(own.dtype),
                gathered,
                shard,
            ),
        )

    return lax.fori_loop(0, place, one, state)


def causal_conv(signal, before, tap_weights):
    tap_count = tap_weights.shape[0]
    row_count = signal.shape[0]
    padded = jnp.concatenate([before, signal], axis=0).astype(jnp.float32)
    running = jnp.zeros(signal.shape, jnp.float32)
    for tap_index in range(tap_count):
        running = (
            running
            + tap_weights[tap_index].astype(jnp.float32) * padded[tap_index : tap_index + row_count]
        )
    return running


def layer_norm(values, scales):
    row_mean = jnp.mean(values, axis=-1, keepdims=True)
    centred = values - row_mean
    spread = jnp.mean(centred * centred, axis=-1, keepdims=True)
    return centred * lax.rsqrt(spread + EPSILON) * scales


def combine_states(earlier_pair, later_pair):
    return (
        earlier_pair[0] * later_pair[1][..., None, None] + later_pair[0],
        earlier_pair[1] * later_pair[1],
    )


def chain_step(state_now, inputs):
    fresh_one, decay_one = inputs
    return (state_now * decay_one[..., None, None] + fresh_one, state_now)


def plain_shards(
    incoming_residual_stream,
    result_valve,
    channel_feed_matrix,
    memory_feed_matrix,
    memory_query_matrix,
    unsoftened_deltas,
    delta_offset,
    channel_fading_speed,
    extra_log_fading,
    bypass_factor,
    channel_feed_kernel,
    memory_feed_kernel,
    memory_query_kernel,
    cluster_scaling_vector,
    mixer_result_matrix,
    initial_scaling_vector,
    valve_matrix,
    widen_matrix,
    shrink_matrix,
    valve_filter_kernel,
    widen_filter_kernel,
    latter_scaling_vector,
):
    row_count = channel_feed_matrix.shape[0]
    inner_here = channel_feed_matrix.shape[1]
    group_count = memory_feed_matrix.shape[1] // STATE
    group_heads = HEADS // GROUPS
    block_count = row_count // BLOCK
    rim_rows = CONV - 1
    rim_x, rim_b, rim_c = shifted(
        (
            channel_feed_matrix[row_count - rim_rows :],
            memory_feed_matrix[row_count - rim_rows :],
            memory_query_matrix[row_count - rim_rows :],
        ),
        "sp",
        1,
    )
    x_act = jax.nn.silu(causal_conv(channel_feed_matrix, rim_x, channel_feed_kernel)).astype(
        jnp.bfloat16
    )
    b_act = jax.nn.silu(causal_conv(memory_feed_matrix, rim_b, memory_feed_kernel)).astype(
        jnp.bfloat16
    )
    c_act = jax.nn.silu(causal_conv(memory_query_matrix, rim_c, memory_query_kernel)).astype(
        jnp.bfloat16
    )
    channel_delta_amount = jax.nn.softplus(unsoftened_deltas + delta_offset[None, :])
    log_fading_amount = extra_log_fading - channel_fading_speed[None, :] * channel_delta_amount
    x_heads = x_act.astype(jnp.float32).reshape(row_count, group_count, group_heads, HEAD_DIM)
    x_scaled = (
        x_heads * channel_delta_amount.reshape(row_count, group_count, group_heads)[..., None]
    )
    b_full = b_act.astype(jnp.float32).reshape(row_count, group_count, STATE)
    c_full = c_act.astype(jnp.float32).reshape(row_count, group_count, STATE)
    decay_full = log_fading_amount.reshape(row_count, group_count, group_heads)
    x_blk = x_scaled.reshape(block_count, BLOCK, group_count, group_heads, HEAD_DIM)
    b_blk = b_full.reshape(block_count, BLOCK, group_count, STATE)
    c_blk = c_full.reshape(block_count, BLOCK, group_count, STATE)
    b_narrow = b_act.reshape(block_count, BLOCK, group_count, STATE)
    c_narrow = c_act.reshape(block_count, BLOCK, group_count, STATE)
    decay_blk = decay_full.reshape(block_count, BLOCK, group_count, group_heads)
    cum_decay = jnp.cumsum(decay_blk, axis=1)
    causal = jnp.tril(jnp.ones((BLOCK, BLOCK), dtype=bool))
    between = cum_decay[:, :, None] - cum_decay[:, None, :]
    lag = jnp.exp(jnp.where(causal[None, :, :, None, None], between, -jnp.inf))
    affinity = jnp.einsum("blgn,bsgn->blsg", c_narrow, b_narrow, preferred_element_type=jnp.float32)
    mixing = affinity[..., None] * lag
    within = jnp.einsum("blsgh,bsghp->blghp", mixing, x_blk, precision=HIGHEST)
    to_end = jnp.exp(cum_decay[:, -1:] - cum_decay)
    fresh = jnp.einsum("blgn,blghp->bghpn", b_blk, x_blk * to_end[..., None], precision=HIGHEST)
    block_decay = jnp.exp(cum_decay[:, -1])
    initial = jnp.zeros((group_count, group_heads, HEAD_DIM, STATE), jnp.float32)
    local_end, earlier = lax.scan(chain_step, initial, (fresh, block_decay))
    carried = (
        jnp.einsum("blgn,bghpn->blghp", c_blk, earlier, precision=HIGHEST)
        * jnp.exp(cum_decay)[..., None]
    )
    from_start = jnp.cumsum(decay_full, axis=0)
    incoming, _ = entering(
        (local_end, jnp.exp(from_start[-1])),
        "sp",
        combine_states,
        (jnp.zeros_like(local_end), jnp.ones_like(from_start[-1])),
    )
    arriving = (
        jnp.einsum("tgn,ghpn->tghp", c_full, incoming, precision=HIGHEST)
        * jnp.exp(from_start)[..., None]
    )
    y_heads = (within + carried).reshape(row_count, group_count, group_heads, HEAD_DIM) + arriving
    y_heads = y_heads + bypass_factor.reshape(group_count, group_heads)[None, :, :, None] * x_heads
    gated = y_heads.reshape(row_count, group_count, group_heads * HEAD_DIM)
    gated = gated * jax.nn.silu(result_valve.astype(jnp.float32)).reshape(
        row_count, group_count, group_heads * HEAD_DIM
    )
    gated = gated * lax.rsqrt(jnp.mean(gated * gated, axis=-1, keepdims=True) + EPSILON)
    y_norm = (gated.reshape(row_count, inner_here) * cluster_scaling_vector[None, :]).astype(
        jnp.bfloat16
    )
    mixer = lax.psum_scatter(
        jnp.dot(y_norm, mixer_result_matrix, preferred_element_type=jnp.float32).astype(
            jnp.bfloat16
        ),
        "tp",
        scatter_dimension=0,
        tiled=True,
    ).astype(jnp.float32)
    normed_own = layer_norm(
        ALPHA * incoming_residual_stream.astype(jnp.float32) + mixer, initial_scaling_vector
    ).astype(jnp.bfloat16)
    normed_all = lax.all_gather(normed_own, "tp", axis=0, tiled=True)
    gate_sum = jnp.dot(
        normed_all,
        lax.all_gather(valve_matrix, "sp", axis=0, tiled=True),
        preferred_element_type=jnp.float32,
    )
    up_sum = jnp.dot(
        normed_all,
        lax.all_gather(widen_matrix, "sp", axis=0, tiled=True),
        preferred_element_type=jnp.float32,
    )
    gate_proj = gate_sum.astype(jnp.bfloat16)
    up_proj = up_sum.astype(jnp.bfloat16)
    ffn_rows = FCONV - 1
    rim_gate, rim_up = shifted(
        (gate_proj[row_count - ffn_rows :], up_proj[row_count - ffn_rows :]), "sp", 1
    )
    gate_conv = causal_conv(gate_proj, rim_gate, valve_filter_kernel)
    up_conv = causal_conv(up_proj, rim_up, widen_filter_kernel)
    hidden = (jax.nn.silu(gate_conv) * up_conv).astype(jnp.bfloat16)
    channel_part = jnp.dot(
        hidden,
        lax.all_gather(shrink_matrix, "sp", axis=1, tiled=True),
        preferred_element_type=jnp.float32,
    )
    channel = lax.psum_scatter(
        channel_part.astype(jnp.bfloat16), "tp", scatter_dimension=0, tiled=True
    ).astype(jnp.float32)
    return layer_norm(
        ALPHA * normed_own.astype(jnp.float32) + channel, latter_scaling_vector
    ).astype(jnp.bfloat16)


MESH = pl.DeviceIdType.MESH
RIM = 16


def silu(v):
    return v / (1.0 + jnp.exp(-v))


def layer_kernel(
    n_sp,
    n_tp,
    res_hbm,
    rv_hbm,
    xf_ref,
    bf_ref,
    cf_ref,
    dt_ref,
    doff_ref,
    fade_ref,
    elf_ref,
    byp_ref,
    xk_ref,
    bk_ref,
    ck_ref,
    csv_ref,
    mm_hbm,
    g1_ref,
    v_hbm,
    w_hbm,
    s_hbm,
    vk_ref,
    wk_ref,
    g2_ref,
    out_ref,
    v_all,
    w_all,
    s_all,
    rim_x,
    rim_b,
    rim_c,
    ext,
    x_act,
    b_act,
    c_act,
    step_ref,
    ld_ref,
    y_ref,
    efs_ref,
    base_ref,
    state_ref,
    st_send,
    dec_send,
    pair_send,
    pair_dec,
    st_recv,
    dec_recv,
    part,
    recv1,
    recv2,
    normed,
    hidden,
    res_ref,
    rv_ref,
    mm_ref,
    late_sem,
    own_sem,
    ring_send,
    ring_recv,
    rim_send,
    rim_recv,
    st_ssem,
    st_rsem,
    t1_send,
    t1_recv,
    t2_send,
    t2_recv,
    t3_send,
    t3_recv,
    nr_send,
    nr_recv,
):
    f32, bf16 = jnp.float32, jnp.bfloat16
    rows, inner = xf_ref.shape
    heads = dt_ref.shape[0]
    own_rows = rows // n_tp
    width = mm_hbm.shape[1]
    ff = v_hbm.shape[1]
    depth = v_hbm.shape[0]
    cols = s_hbm.shape[1]
    blocks = rows // BLOCK
    me = lax.axis_index("sp")
    mt = lax.axis_index("tp")
    half = n_sp // 2

    def owner(pos):
        back = pos // half
        return (1 - back) * 2 * pos + back * (2 * (n_sp - 1 - pos) + 1)

    odd = me % 2
    place = (1 - odd) * (me // 2) + odd * (n_sp - 1 - me // 2)
    after = owner((place + 1) % n_sp)
    ahead = owner((place + n_sp - 1) % n_sp)

    barrier = pltpu.get_barrier_semaphore()
    for d in range(1, n_sp):
        pl.semaphore_signal(barrier, inc=1, device_id=((me + d) % n_sp, mt), device_id_type=MESH)
    for d in range(1, n_tp):
        pl.semaphore_signal(barrier, inc=1, device_id=(me, (mt + d) % n_tp), device_id_type=MESH)
    pl.semaphore_wait(barrier, n_sp + n_tp - 2)

    def slot(piece, who):
        if piece == 2:
            return s_all.at[who]
        whole = v_all if piece == 0 else w_all
        return whole.at[pl.ds(pl.multiple_of(who * depth, depth), depth)]

    sources = (v_hbm, w_hbm, s_hbm)
    hops = {}
    for piece in range(3):
        long_way = half if piece != 1 else n_sp - 1 - half
        hops[piece] = (long_way, n_sp - 1 - long_way) if piece < 2 else (half, half)

    def ring_copy(piece, way, step):
        who = owner((place + n_sp - step) % n_sp if way == 0 else (place + step) % n_sp)
        src = sources[piece] if step == 0 else slot(piece, who)
        dst = slot(piece, who)
        if piece == 2 and step == half - 1:
            part_rows = src.shape[0] // 2
            here = pl.ds(way * part_rows, part_rows)
            src, dst = src.at[here], dst.at[here]
        return pltpu.make_async_remote_copy(
            src_ref=src,
            dst_ref=dst,
            send_sem=ring_send.at[way, step, piece],
            recv_sem=ring_recv.at[way, step, piece],
            device_id=(after if way == 0 else ahead, mt),
            device_id_type=MESH,
        )

    def advance(piece, step):
        for way in range(2):
            if 1 <= step <= hops[piece][way]:
                ring_copy(piece, way, step - 1).wait_recv()
            if step < hops[piece][way]:
                ring_copy(piece, way, step).start()

    rim_copies = []
    for i, (a, b) in enumerate(((xf_ref, rim_x), (bf_ref, rim_b), (cf_ref, rim_c))):
        rim_copies.append(
            pltpu.make_async_remote_copy(
                src_ref=a.at[pl.ds(rows - RIM, RIM)],
                dst_ref=b,
                send_sem=rim_send.at[i],
                recv_sem=rim_recv.at[i],
                device_id=((me + 1) % n_sp, mt),
                device_id_type=MESH,
            )
        )
        rim_copies[-1].start()
    own_copies = []
    for piece in range(3):
        if piece < 2:
            advance(piece, 0)
        own_copies.append(
            pltpu.make_async_copy(sources[piece], slot(piece, me), own_sem.at[piece])
        )
        own_copies[-1].start()

    late = [
        pltpu.make_async_copy(a, b, late_sem.at[i])
        for i, (a, b) in enumerate(((rv_hbm, rv_ref), (mm_hbm, mm_ref), (res_hbm, res_ref)))
    ]
    for c in late:
        c.start()

    eye = lax.broadcasted_iota(jnp.int32, (heads, heads), 0) == lax.broadcasted_iota(
        jnp.int32, (heads, heads), 1
    )

    def column(a):
        return jnp.sum(jnp.where(eye, a[...], 0.0), axis=1, keepdims=True)

    raw = dt_ref[...] + column(doff_ref)
    step_ref[...] = jnp.maximum(raw, 0.0) + jnp.log1p(jnp.exp(-jnp.abs(raw)))
    ld_ref[...] = elf_ref[...] - column(fade_ref) * step_ref[...]

    for c in rim_copies:
        c.wait_recv()
    first = me == 0
    for rim, feed, taps, act in (
        (rim_x, xf_ref, xk_ref, x_act),
        (rim_b, bf_ref, bk_ref, b_act),
        (rim_c, cf_ref, ck_ref, c_act),
    ):
        for lo in range(0, feed.shape[1], 128):
            here = slice(lo, lo + 128)
            edge = rim[:, here].astype(f32)
            ext[0:RIM, :] = jnp.where(first, jnp.zeros_like(edge), edge)
            ext[RIM:, :] = feed[:, here].astype(f32)
            tap = taps[:, here].astype(f32)
            total = jnp.zeros((rows, 128), f32)
            for k in range(CONV):
                start = RIM - (CONV - 1) + k
                total = total + tap[k : k + 1] * ext[start : start + rows, :]
            act[:, here] = silu(total).astype(bf16)

    li = lax.broadcasted_iota(jnp.int32, (BLOCK, BLOCK), 0)
    si = lax.broadcasted_iota(jnp.int32, (BLOCK, BLOCK), 1)
    causal = li >= si
    lower = jnp.where(causal, 1.0, 0.0).astype(f32)
    upper = jnp.where(li <= si, 1.0, 0.0).astype(f32)
    spread = jnp.where(
        lax.broadcasted_iota(jnp.int32, (heads, inner), 1) // HEAD_DIM
        == lax.broadcasted_iota(jnp.int32, (heads, inner), 0),
        1.0,
        0.0,
    ).astype(f32)
    near = lax.broadcasted_iota(jnp.int32, (BLOCK, 2 * HEAD_DIM), 1) < HEAD_DIM

    def widen(a):
        return jnp.dot(a, spread, precision=HIGHEST, preferred_element_type=f32)

    state_ref[...] = jnp.zeros_like(state_ref)
    base_ref[...] = jnp.zeros_like(base_ref)
    skip = widen(byp_ref[...])

    def scan_block(b, carry):
        at = pl.ds(pl.multiple_of(b * BLOCK, BLOCK), BLOCK)
        ld = ld_ref[:, at]
        cum = lax.dot_general(
            lower, ld, (((1,), (1,)), ((), ())), precision=HIGHEST, preferred_element_type=f32
        )
        cum_t = jnp.dot(ld, upper, precision=HIGHEST, preferred_element_type=f32)
        last = cum[BLOCK - 1 : BLOCK, :]
        x = x_act[at, :].astype(f32)
        bb = b_act[at, :]
        cc = c_act[at, :]
        xs = x * lax.dot_general(
            step_ref[:, at],
            spread,
            (((0,), (0,)), ((), ())),
            precision=HIGHEST,
            preferred_element_type=f32,
        )
        xs16 = xs.astype(bf16)
        aff = lax.dot_general(
            cc, bb, (((1,), (1,)), ((), ())), preferred_element_type=f32
        )
        y = (
            jnp.dot(cc, state_ref[...].astype(bf16), preferred_element_type=f32)
            * widen(jnp.exp(cum))
            + skip * x
        )
        for pair in range(heads // 2):
            at_pair = slice(pair * 2 * HEAD_DIM, (pair + 1) * 2 * HEAD_DIM)
            both = []
            for h in (2 * pair, 2 * pair + 1):
                gap = cum[:, h : h + 1] - cum_t[h : h + 1, :]
                lag = jnp.exp(jnp.where(causal, gap, -1e30))
                both.append(
                    jnp.dot(
                        (aff * lag).astype(bf16), xs16[:, at_pair], preferred_element_type=f32
                    )
                )
            y_ref[at, at_pair] = y[:, at_pair] + jnp.where(near, both[0], both[1])
        fresh = lax.dot_general(
            bb,
            (xs * widen(jnp.exp(last - cum))).astype(bf16),
            (((0,), (0,)), ((), ())),
            preferred_element_type=f32,
        )
        state_ref[...] = state_ref[...] * widen(jnp.exp(last)) + fresh
        base = base_ref[0:1, :]
        efs_ref[at, :] = jnp.exp(base + cum)
        base_ref[0:1, :] = base + last
        return carry

    lax.fori_loop(0, blocks, scan_block, 0)
    st_send[...] = state_ref[...].astype(bf16)
    dec_send[...] = jnp.broadcast_to(base_ref[0:1, :], dec_send.shape)
    partner = me + 1 - 2 * odd

    def state_copies(d):
        pair = d > 0
        return [
            pltpu.make_async_remote_copy(
                src_ref=a,
                dst_ref=b.at[d],
                send_sem=st_ssem.at[d, i],
                recv_sem=st_rsem.at[d, i],
                device_id=((me + 2 * d) % n_sp if pair else partner, mt),
                device_id_type=MESH,
            )
            for i, (a, b) in enumerate(
                ((pair_send if pair else st_send, st_recv), (pair_dec if pair else dec_send, dec_recv))
            )
        ]

    for c in state_copies(0):
        c.start()
    advance(0, 1)
    for c in state_copies(0):
        c.wait_recv()
    own_dec = widen(jnp.exp(dec_send[0:1, :]))
    beside_dec = widen(jnp.exp(dec_recv[0, 0:1, :]))
    beside = st_recv[0].astype(f32)
    later = odd == 1
    pair_send[...] = jnp.where(
        later, state_ref[...] + beside * own_dec, state_ref[...] * beside_dec + beside
    ).astype(bf16)
    pair_dec[...] = dec_send[...] + dec_recv[0]
    state_ref[...] = jnp.zeros_like(state_ref)
    for d in range(1, half):

        @pl.when(me + 2 * d < n_sp)
        def _(d=d):
            for c in state_copies(d):
                c.start()

    advance(1, 1)
    advance(2, 0)
    for d in range(half - 1, 0, -1):

        @pl.when(me >= 2 * d)
        def _(d=d):
            for c in state_copies(d):
                c.wait_recv()
            state_ref[...] = state_ref[...] * widen(
                jnp.exp(dec_recv[d, 0:1, :])
            ) + st_recv[d].astype(f32)

    @pl.when(odd == 1)
    def _():
        state_ref[...] = state_ref[...] * widen(jnp.exp(dec_recv[0, 0:1, :])) + st_recv[
            0
        ].astype(f32)

    for c in late:
        c.wait()

    def project_block(b, carry):
        at = pl.ds(pl.multiple_of(b * BLOCK, BLOCK), BLOCK)
        y = y_ref[at, :] + jnp.dot(
            c_act[at, :], state_ref[...].astype(bf16), preferred_element_type=f32
        ) * widen(efs_ref[at, :])
        gated = y * silu(rv_ref[at, :].astype(f32))
        gated = gated * lax.rsqrt(jnp.mean(gated * gated, axis=-1, keepdims=True) + EPSILON)
        y_norm = (gated * csv_ref[...]).astype(bf16)
        part[at, :] = jnp.dot(y_norm, mm_ref[...], preferred_element_type=f32).astype(bf16)
        return carry

    lax.fori_loop(0, blocks, project_block, 0)

    def rows_of(t):
        return pl.ds(pl.multiple_of(t * own_rows, own_rows), own_rows)

    def tp_copy(d, src, dst, send, recv):
        return pltpu.make_async_remote_copy(
            src_ref=src,
            dst_ref=dst,
            send_sem=send,
            recv_sem=recv,
            device_id=(me, (mt + d) % n_tp),
            device_id_type=MESH,
        )

    first_sum = [
        tp_copy(d, part.at[rows_of((mt + d) % n_tp)], recv1.at[d], t1_send.at[d], t1_recv.at[d])
        for d in range(1, n_tp)
    ]
    for c in first_sum:
        c.start()
    advance(0, 2)
    for c in first_sum:
        c.wait_recv()
    mixer = part[rows_of(mt), :].astype(f32)
    for d in range(1, n_tp):
        mixer = mixer + recv1[d].astype(f32)
    mine = pl.ds(pl.multiple_of(RIM + mt * own_rows, RIM), own_rows)
    normed[mine, :] = layer_norm(
        ALPHA * res_ref[...].astype(f32) + mixer, g1_ref[...]
    ).astype(bf16)
    for c in first_sum:
        c.wait_send()
    spread_rows = [
        tp_copy(d, normed.at[mine], normed.at[mine], t2_send.at[d], t2_recv.at[d])
        for d in range(1, n_tp)
    ]
    for c in spread_rows:
        c.start()
    advance(1, 2)
    advance(0, 3)
    for c in spread_rows:
        c.wait()
    rim_norm = pltpu.make_async_remote_copy(
        src_ref=normed.at[pl.ds(rows, RIM)],
        dst_ref=normed.at[pl.ds(0, RIM)],
        send_sem=nr_send,
        recv_sem=nr_recv,
        device_id=((me + 1) % n_sp, mt),
        device_id_type=MESH,
    )

    @pl.when(me + 1 < n_sp)
    def _():
        rim_norm.start()

    @pl.when(me == 0)
    def _():
        normed[0:RIM, :] = jnp.zeros((RIM, width), bf16)

    advance(1, 3)
    advance(2, 1)
    for s in range(4, half + 1):
        advance(0, s)
        advance(1, s)

    @pl.when(me > 0)
    def _():
        rim_norm.wait_recv()

    for c in own_copies:
        c.wait()

    def ffn_cols(at):
        feeds = normed[...]
        convs = []
        for weights, taps in ((v_all, vk_ref), (w_all, wk_ref)):
            proj = jnp.dot(feeds, weights[:, at], preferred_element_type=f32)
            proj = proj.astype(bf16).astype(f32)
            tap = taps[:, at].astype(f32)
            total = jnp.zeros((rows, proj.shape[1]), f32)
            for k in range(FCONV):
                start = RIM - (FCONV - 1) + k
                total = total + tap[k : k + 1] * proj[start : start + rows, :]
            convs.append(total)
        hidden[:, at] = (silu(convs[0]) * convs[1]).astype(bf16)

    chunk = 256
    full = ff // chunk

    def ffn_chunk(i, carry):
        ffn_cols(pl.ds(pl.multiple_of(i * chunk, chunk), chunk))
        return carry

    lax.fori_loop(0, full // 2, ffn_chunk, 0)
    advance(2, 2)
    lax.fori_loop(full // 2, full, ffn_chunk, 0)
    if ff % chunk:
        ffn_cols(pl.ds(full * chunk, ff % chunk))

    def down(who):
        at = pl.ds(pl.multiple_of(who * cols, cols), cols)
        part[:, at] = jnp.dot(
            hidden[...], s_all[who], preferred_element_type=f32
        ).astype(bf16)

    def down_copies(who):
        at = pl.ds(pl.multiple_of(who * cols, cols), cols)
        return [
            tp_copy(
                d,
                part.at[rows_of((mt + d) % n_tp), at],
                recv2.at[d, :, at],
                t3_send.at[d, who],
                t3_recv.at[d, who],
            )
            for d in range(1, n_tp)
        ]

    down(me)
    for c in down_copies(me):
        c.start()
    for k in range(1, half + 1):
        if k >= 3:
            advance(2, k)
        count = 2 if k < half else 1

        def both_ways(q, carry, k=k):
            who = owner((place + n_sp - k + 2 * k * q) % n_sp)
            down(who)
            for c in down_copies(who):
                c.start()
            return carry

        lax.fori_loop(0, count, both_ways, 0)

    def settle(who, carry):
        for c in down_copies(who):
            c.wait()
        return carry

    lax.fori_loop(0, n_sp, settle, 0)
    channel = part[rows_of(mt), :].astype(f32)
    for d in range(1, n_tp):
        channel = channel + recv2[d].astype(f32)
    out_ref[...] = layer_norm(
        ALPHA * normed[mine, :].astype(f32) + channel, g2_ref[...]
    ).astype(bf16)

    for piece in range(3):
        for way in range(2):
            for s in range(hops[piece][way]):
                ring_copy(piece, way, s).wait_send()
    for c in rim_copies:
        c.wait_send()

    @pl.when(me + 1 < n_sp)
    def _():
        rim_norm.wait_send()

    for c in state_copies(0):
        c.wait_send()
    for d in range(1, half):

        @pl.when(me + 2 * d < n_sp)
        def _(d=d):
            for c in state_copies(d):
                c.wait_send()


def fused_shards(n_sp, n_tp, *args):
    (
        res, rv, xf, bf, cf, dt, doff, fade, elf, byp, xk, bk, ck, csv, mm, g1, v, w, s, vk, wk, g2
    ) = args
    f32, bf16 = jnp.float32, jnp.bfloat16
    rows, inner = xf.shape
    heads = dt.shape[1]
    width = mm.shape[1]
    ff = v.shape[1]
    row = lambda a: a.reshape(1, -1)
    half = n_sp // 2
    vmem = pl.BlockSpec(memory_space=pltpu.VMEM)
    hbm = pl.BlockSpec(memory_space=pl.ANY)
    dma = pltpu.SemaphoreType.DMA
    return pl.pallas_call(
        functools.partial(layer_kernel, n_sp, n_tp),
        out_shape=jax.ShapeDtypeStruct(res.shape, bf16),
        in_specs=[hbm] * 2 + [vmem] * 12 + [hbm, vmem] + [hbm] * 3 + [vmem] * 3,
        out_specs=vmem,
        scratch_shapes=[
            pltpu.VMEM((n_sp * v.shape[0], ff), bf16),
            pltpu.VMEM((n_sp * v.shape[0], ff), bf16),
            pltpu.VMEM((n_sp,) + s.shape, bf16),
            pltpu.VMEM((RIM, inner), bf16),
            pltpu.VMEM((RIM, STATE), bf16),
            pltpu.VMEM((RIM, STATE), bf16),
            pltpu.VMEM((rows + RIM, 128), f32),
            pltpu.VMEM((rows, inner), bf16),
            pltpu.VMEM((rows, STATE), bf16),
            pltpu.VMEM((rows, STATE), bf16),
            pltpu.VMEM((heads, rows), f32),
            pltpu.VMEM((heads, rows), f32),
            pltpu.VMEM((rows, inner), f32),
            pltpu.VMEM((rows, heads), f32),
            pltpu.VMEM((8, heads), f32),
            pltpu.VMEM((STATE, inner), f32),
            pltpu.VMEM((STATE, inner), bf16),
            pltpu.VMEM((8, heads), f32),
            pltpu.VMEM((STATE, inner), bf16),
            pltpu.VMEM((8, heads), f32),
            pltpu.VMEM((half, STATE, inner), bf16),
            pltpu.VMEM((half, 8, heads), f32),
            pltpu.VMEM((rows, width), bf16),
            pltpu.VMEM((n_tp, rows // n_tp, width), bf16),
            pltpu.VMEM((n_tp, rows // n_tp, width), bf16),
            pltpu.VMEM((rows + RIM, width), bf16),
            pltpu.VMEM((rows, ff), bf16),
            pltpu.VMEM(res.shape, bf16),
            pltpu.VMEM(rv.shape, bf16),
            pltpu.VMEM(mm.shape, bf16),
            dma((3,)),
            dma((3,)),
            dma((2, half, 3)),
            dma((2, half, 3)),
            dma((3,)),
            dma((3,)),
            dma((half, 2)),
            dma((half, 2)),
            dma((n_tp,)),
            dma((n_tp,)),
            dma((n_tp,)),
            dma((n_tp,)),
            dma((n_tp, n_sp)),
            dma((n_tp, n_sp)),
            dma,
            dma,
        ],
        compiler_params=pltpu.CompilerParams(
            collective_id=0, has_side_effects=True, vmem_limit_bytes=60 * 1024 * 1024
        ),
    )(
        res, rv, xf, bf, cf, dt.T, row(doff), row(fade), elf.T, row(byp), xk, bk, ck, row(csv), mm,
        row(g1), v, w, s, vk, wk, row(g2),
    )


def shards_for(n_sp, n_tp):
    def shards(*args):
        rows = args[2].shape[0]
        fits = (
            args[3].shape[1] == STATE
            and args[18].shape[1] % 128 == 0
            and args[16].shape[0] % 16 == 0
            and args[16].shape[1] % 128 == 0
            and n_sp % 2 == 0
            and n_sp >= 4
            and args[18].shape[0] % 32 == 0
            and rows % (BLOCK * n_tp) == 0
        )
        if fits:
            return fused_shards(n_sp, n_tp, *args)
        return plain_shards(*args)

    return shards


def solution(mesh):
    in_specs = (
        P(("sp", "tp"), None),
        P("sp", "tp"),
        P("sp", "tp"),
        P("sp", "tp"),
        P("sp", "tp"),
        P("sp", "tp"),
        P("tp"),
        P("tp"),
        P("sp", "tp"),
        P("tp"),
        P(None, "tp"),
        P(None, "tp"),
        P(None, "tp"),
        P("tp"),
        P("tp", None),
        P(),
        P("sp", "tp"),
        P("sp", "tp"),
        P("tp", "sp"),
        P(None, "tp"),
        P(None, "tp"),
        P(),
    )
    out_specs = P(("sp", "tp"), None)
    shards = shards_for(mesh.shape["sp"], mesh.shape["tp"])
    return jax.shard_map(shards, mesh=mesh, in_specs=in_specs, out_specs=out_specs, check_vma=False)
```

profile of v0, /device:TPU:19, one launch (start us, length us, event | category | flops | bytes accessed | tf_op | source)
XLA Modules:
  0.0 192.8 jit_solution(3608524297670995484)
XLA Ops:
  0.0 190.9 %shard_map.208 = bf16[128,2048]{1,0:T(8,128)(2,1)} custom-call(bf16[128,2048]{1,0:T(8,128)(2,1)} %res_hbm.1, bf16[512,512]{1,0:T(8,128)(2,1)} %rv_hbm.1, bf16[512,512]{1,0:T(8,128)(2,1)} %xf_ref.1, bf16[512,128]{1,0:T(8,128)(2,1)} %bf_ref.1, bf16[512,128]{1,0:T(8,128)(2,1)} %cf_ref.1, f32[8,512]{1,0:T(8,128)} %bitcast.8, f32[1,8]{1,0:T(1,128)} %bitcast.13, ...), custom_call_target="tpu_custom_call" | custom-call | tf_op jit(solution)/shard_map/pallas_call | solution.py:760
  190.9 1.9 copy.24
where the time goes:
time: 193 us
  Pallas kernels  191 us (99%)
    pallas_call x1, Pallas kernels, fused_shards(): pl.pallas_call(functools.partial(layer_kernel, n_sp, n_tp), out_shape=jax...  191 us

commit v1 on v0

--- a/solution.py
+++ b/solution.py
@@ -224,6 +224,8 @@
 
 MESH = pl.DeviceIdType.MESH
 RIM = 16
+FAN = 2
+HALVES = 2
 
 
 def silu(v):
@@ -262,6 +264,8 @@
     rim_x,
     rim_b,
     rim_c,
+    vk_other,
+    wk_other,
     ext,
     x_act,
     b_act,
@@ -279,7 +283,10 @@
     st_recv,
     dec_recv,
     part,
-    recv1,
+    near_recv,
+    side_send,
+    side_recv,
+    own_norm,
     recv2,
     normed,
     hidden,
@@ -288,20 +295,29 @@
     mm_ref,
     late_sem,
     own_sem,
-    ring_send,
-    ring_recv,
+    w_recv,
+    z_send,
+    xo_send,
+    do_send,
+    xr_send,
+    dr_send,
     rim_send,
     rim_recv,
+    tap_send,
+    tap_recv,
     st_ssem,
     st_rsem,
-    t1_send,
-    t1_recv,
-    t2_send,
-    t2_recv,
+    a_send,
+    a_recv,
+    b_send,
+    b_recv,
+    ag_send,
+    ag_recv,
+    agr_send,
+    halo_send,
+    halo_recv,
     t3_send,
     t3_recv,
-    nr_send,
-    nr_recv,
 ):
     f32, bf16 = jnp.float32, jnp.bfloat16
     rows, inner = xf_ref.shape
@@ -312,90 +328,179 @@
     depth = v_hbm.shape[0]
     cols = s_hbm.shape[1]
     blocks = rows // BLOCK
+    planes = n_sp // FAN
+    dests = planes // 2
+    half = n_sp // 2
     me = lax.axis_index("sp")
     mt = lax.axis_index("tp")
-    half = n_sp // 2
-
-    def owner(pos):
-        back = pos // half
-        return (1 - back) * 2 * pos + back * (2 * (n_sp - 1 - pos) + 1)
-
-    odd = me % 2
-    place = (1 - odd) * (me // 2) + odd * (n_sp - 1 - me // 2)
-    after = owner((place + 1) % n_sp)
-    ahead = owner((place + n_sp - 1) % n_sp)
+    z, x = me // FAN, me % FAN
+    y, c = mt // 2, mt % 2
+    b = z % 2
+    mate = z + 1 - 2 * b
+    pair0 = z - b
+
+    def dev(pz, px, py, pc):
+        return (pz * FAN + px, py * 2 + pc)
+
+    def remote(src, dst, send, recv, device):
+        return pltpu.make_async_remote_copy(
+            src_ref=src, dst_ref=dst, send_sem=send, recv_sem=recv, device_id=device, device_id_type=MESH
+        )
 
     barrier = pltpu.get_barrier_semaphore()
-    for d in range(1, n_sp):
-        pl.semaphore_signal(barrier, inc=1, device_id=((me + d) % n_sp, mt), device_id_type=MESH)
-    for d in range(1, n_tp):
-        pl.semaphore_signal(barrier, inc=1, device_id=(me, (mt + d) % n_tp), device_id_type=MESH)
-    pl.semaphore_wait(barrier, n_sp + n_tp - 2)
-
-    def slot(piece, who):
-        if piece == 2:
-            return s_all.at[who]
-        whole = v_all if piece == 0 else w_all
-        return whole.at[pl.ds(pl.multiple_of(who * depth, depth), depth)]
-
+    total_devices = n_sp * n_tp
+    line = me * n_tp + mt
+    for d in range(1, total_devices):
+        who = (line + d) % total_devices
+        pl.semaphore_signal(barrier, inc=1, device_id=(who // n_tp, who % n_tp), device_id_type=MESH)
+    pl.semaphore_wait(barrier, total_devices - 1)
+
+    units = [(kind, g) for kind in range(3) for g in range(HALVES)]
     sources = (v_hbm, w_hbm, s_hbm)
-    hops = {}
-    for piece in range(3):
-        long_way = half if piece != 1 else n_sp - 1 - half
-        hops[piece] = (long_way, n_sp - 1 - long_way) if piece < 2 else (half, half)
-
-    def ring_copy(piece, way, step):
-        who = owner((place + n_sp - step) % n_sp if way == 0 else (place + step) % n_sp)
-        src = sources[piece] if step == 0 else slot(piece, who)
-        dst = slot(piece, who)
-        if piece == 2 and step == half - 1:
-            part_rows = src.shape[0] // 2
-            here = pl.ds(way * part_rows, part_rows)
-            src, dst = src.at[here], dst.at[here]
-        return pltpu.make_async_remote_copy(
-            src_ref=src,
-            dst_ref=dst,
-            send_sem=ring_send.at[way, step, piece],
-            recv_sem=ring_recv.at[way, step, piece],
-            device_id=(after if way == 0 else ahead, mt),
-            device_id_type=MESH,
-        )
-
-    def advance(piece, step):
-        for way in range(2):
-            if 1 <= step <= hops[piece][way]:
-                ring_copy(piece, way, step - 1).wait_recv()
-            if step < hops[piece][way]:
-                ring_copy(piece, way, step).start()
+
+    def place(u, q):
+        kind, g = units[u]
+        size = (ff if kind == 2 else depth) // (2 * HALVES)
+        return size, (q * HALVES + g) * size
+
+    def own_piece(u, q):
+        size, at = place(u, q)
+        return sources[units[u][0]].at[pl.ds(pl.multiple_of(at, 16), size)]
+
+    def slot(u, q, who):
+        size, at = place(u, q)
+        kind = units[u][0]
+        if kind == 2:
+            return s_all.at[who, pl.ds(pl.multiple_of(at, 16), size)]
+        whole = v_all if kind == 0 else w_all
+        return whole.at[pl.ds(pl.multiple_of(who * depth + at, 16), size)]
+
+    def landed(u, q, who):
+        here = slot(u, q, who)
+        return remote(here, here, do_send.at[0, 0], w_recv.at[u, q, who], dev(z, x, y, 1 - c))
+
+    def z_copy(u, q, j):
+        return remote(
+            own_piece(u, q),
+            slot(u, q, me),
+            z_send.at[u, q, j],
+            w_recv.at[u, q, me],
+            dev(2 * j + c, x, y, q),
+        )
+
+    def xo_copy(u, q):
+        return remote(
+            own_piece(u, q), slot(u, q, me), xo_send.at[u, q], w_recv.at[u, q, me], dev(z, 1 - x, y, q)
+        )
+
+    def do_copy(u, q):
+        return remote(
+            own_piece(u, q), slot(u, q, me), do_send.at[u, q], w_recv.at[u, q, me], dev(z, x, y, 1 - c)
+        )
+
+    def xr_copy(u, i):
+        here = slot(u, c, plane_at(i) * FAN + x)
+        return remote(
+            here,
+            here,
+            xr_send.at[u, i],
+            w_recv.at[u, c, plane_at(i) * FAN + x],
+            dev(z, 1 - x, y, c),
+        )
+
+    def dr_copy(u, who):
+        here = slot(u, c, who)
+        return remote(here, here, dr_send.at[u, who], w_recv.at[u, c, who], dev(z, x, y, 1 - c))
+
+    def plane_at(i):
+        if i == 0:
+            return z
+        low = jnp.where(z < planes // 2, z, planes - 1 - z)
+        got = jnp.where(i - 1 < low, i - 1, i)
+        return jnp.where(z < planes // 2, got, planes - 1 - got)
+
+    def send_z(which):
+        for u in which:
+            for q in range(2):
+                for j in range(dests):
+
+                    @pl.when(2 * j + c != z)
+                    def _(u=u, q=q, j=j):
+                        z_copy(u, q, j).start()
+
+    def send_xo(which):
+        @pl.when(c == b)
+        def _():
+            for u in which:
+                for q in range(2):
+                    xo_copy(u, q).start()
+
+    def relay_col(u, picks=None):
+        for i in picks or range(1, planes):
+            who = plane_at(i) * FAN + x
+            landed(u, c, who).wait_recv()
+            xr_copy(u, i).start()
+            dr_copy(u, who).start()
+
+    def relay_x(u, picks=None):
+        for i in picks or range(planes):
+            who = plane_at(i) * FAN + 1 - x
+            landed(u, c, who).wait_recv()
+            dr_copy(u, who).start()
+
+    def other_half(us, who):
+        for u in us:
+            landed(u, 1 - c, who).wait_recv()
+
+    def own_block(us):
+        @pl.when(c != b)
+        def _():
+            for u in us:
+                for q in range(2):
+                    landed(u, q, me).wait_recv()
 
     rim_copies = []
-    for i, (a, b) in enumerate(((xf_ref, rim_x), (bf_ref, rim_b), (cf_ref, rim_c))):
+    for i, (src, dst) in enumerate(((xf_ref, rim_x), (bf_ref, rim_b), (cf_ref, rim_c))):
         rim_copies.append(
-            pltpu.make_async_remote_copy(
-                src_ref=a.at[pl.ds(rows - RIM, RIM)],
-                dst_ref=b,
-                send_sem=rim_send.at[i],
-                recv_sem=rim_recv.at[i],
-                device_id=((me + 1) % n_sp, mt),
-                device_id_type=MESH,
+            remote(
+                src.at[pl.ds(rows - RIM, RIM)],
+                dst,
+                rim_send.at[i],
+                rim_recv.at[i],
+                ((me + 1) % n_sp, mt),
             )
         )
         rim_copies[-1].start()
+    tap_copies = [
+        remote(src, dst, tap_send.at[i], tap_recv.at[i], dev(z, x, y, 1 - c))
+        for i, (src, dst) in enumerate(((vk_ref, vk_other), (wk_ref, wk_other)))
+    ]
+    for copy in tap_copies:
+        copy.start()
+    send_z([0])
+    send_xo([0, 1, 2, 3])
+
     own_copies = []
-    for piece in range(3):
-        if piece < 2:
-            advance(piece, 0)
-        own_copies.append(
-            pltpu.make_async_copy(sources[piece], slot(piece, me), own_sem.at[piece])
-        )
-        own_copies[-1].start()
+    for kind in range(3):
+        dst = s_all.at[me] if kind == 2 else (v_all, w_all)[kind].at[
+            pl.ds(pl.multiple_of(me * depth, 16), depth)
+        ]
+        own_copies.append(pltpu.make_async_copy(sources[kind], dst, own_sem.at[kind]))
+
+    @pl.when(c == b)
+    def _():
+        for u in range(len(units)):
+            for q in range(2):
+                do_copy(u, q).start()
+        for copy in own_copies:
+            copy.start()
 
     late = [
-        pltpu.make_async_copy(a, b, late_sem.at[i])
-        for i, (a, b) in enumerate(((rv_hbm, rv_ref), (mm_hbm, mm_ref), (res_hbm, res_ref)))
+        pltpu.make_async_copy(src, dst, late_sem.at[i])
+        for i, (src, dst) in enumerate(((rv_hbm, rv_ref), (mm_hbm, mm_ref), (res_hbm, res_ref)))
     ]
-    for c in late:
-        c.start()
+    for copy in late:
+        copy.start()
 
     eye = lax.broadcasted_iota(jnp.int32, (heads, heads), 0) == lax.broadcasted_iota(
         jnp.int32, (heads, heads), 1
@@ -408,8 +513,8 @@
     step_ref[...] = jnp.maximum(raw, 0.0) + jnp.log1p(jnp.exp(-jnp.abs(raw)))
     ld_ref[...] = elf_ref[...] - column(fade_ref) * step_ref[...]
 
-    for c in rim_copies:
-        c.wait_recv()
+    for copy in rim_copies:
+        copy.wait_recv()
     first = me == 0
     for rim, feed, taps, act in (
         (rim_x, xf_ref, xk_ref, x_act),
@@ -448,18 +553,18 @@
     base_ref[...] = jnp.zeros_like(base_ref)
     skip = widen(byp_ref[...])
 
-    def scan_block(b, carry):
-        at = pl.ds(pl.multiple_of(b * BLOCK, BLOCK), BLOCK)
+    def scan_block(i, carry):
+        at = pl.ds(pl.multiple_of(i * BLOCK, BLOCK), BLOCK)
         ld = ld_ref[:, at]
         cum = lax.dot_general(
             lower, ld, (((1,), (1,)), ((), ())), precision=HIGHEST, preferred_element_type=f32
         )
         cum_t = jnp.dot(ld, upper, precision=HIGHEST, preferred_element_type=f32)
         last = cum[BLOCK - 1 : BLOCK, :]
-        x = x_act[at, :].astype(f32)
+        xx = x_act[at, :].astype(f32)
         bb = b_act[at, :]
         cc = c_act[at, :]
-        xs = x * lax.dot_general(
+        xs = xx * lax.dot_general(
             step_ref[:, at],
             spread,
             (((0,), (0,)), ((), ())),
@@ -470,10 +575,10 @@
         aff = lax.dot_general(
             cc, bb, (((1,), (1,)), ((), ())), preferred_element_type=f32
         )
-        y = (
+        yy = (
             jnp.dot(cc, state_ref[...].astype(bf16), preferred_element_type=f32)
             * widen(jnp.exp(cum))
-            + skip * x
+            + skip * xx
         )
         for pair in range(heads // 2):
             at_pair = slice(pair * 2 * HEAD_DIM, (pair + 1) * 2 * HEAD_DIM)
@@ -486,7 +591,7 @@
                         (aff * lag).astype(bf16), xs16[:, at_pair], preferred_element_type=f32
                     )
                 )
-            y_ref[at, at_pair] = y[:, at_pair] + jnp.where(near, both[0], both[1])
+            y_ref[at, at_pair] = yy[:, at_pair] + jnp.where(near, both[0], both[1])
         fresh = lax.dot_general(
             bb,
             (xs * widen(jnp.exp(last - cum))).astype(bf16),
@@ -502,29 +607,29 @@
     lax.fori_loop(0, blocks, scan_block, 0)
     st_send[...] = state_ref[...].astype(bf16)
     dec_send[...] = jnp.broadcast_to(base_ref[0:1, :], dec_send.shape)
+    odd = me % 2
     partner = me + 1 - 2 * odd
 
     def state_copies(d):
         pair = d > 0
         return [
-            pltpu.make_async_remote_copy(
-                src_ref=a,
-                dst_ref=b.at[d],
-                send_sem=st_ssem.at[d, i],
-                recv_sem=st_rsem.at[d, i],
-                device_id=((me + 2 * d) % n_sp if pair else partner, mt),
-                device_id_type=MESH,
+            remote(
+                src,
+                dst.at[d],
+                st_ssem.at[d, i],
+                st_rsem.at[d, i],
+                ((me + 2 * d) % n_sp if pair else partner, mt),
             )
-            for i, (a, b) in enumerate(
+            for i, (src, dst) in enumerate(
                 ((pair_send if pair else st_send, st_recv), (pair_dec if pair else dec_send, dec_recv))
             )
         ]
 
-    for c in state_copies(0):
-        c.start()
-    advance(0, 1)
-    for c in state_copies(0):
-        c.wait_recv()
+    for copy in state_copies(0):
+        copy.start()
+    send_xo([4, 5])
+    for copy in state_copies(0):
+        copy.wait_recv()
     own_dec = widen(jnp.exp(dec_send[0:1, :]))
     beside_dec = widen(jnp.exp(dec_recv[0, 0:1, :]))
     beside = st_recv[0].astype(f32)
@@ -538,17 +643,17 @@
 
         @pl.when(me + 2 * d < n_sp)
         def _(d=d):
-            for c in state_copies(d):
-                c.start()
-
-    advance(1, 1)
-    advance(2, 0)
+            for copy in state_copies(d):
+                copy.start()
+
+    send_z([1, 2])
+    relay_col(0)
     for d in range(half - 1, 0, -1):
 
         @pl.when(me >= 2 * d)
         def _(d=d):
-            for c in state_copies(d):
-                c.wait_recv()
+            for copy in state_copies(d):
+                copy.wait_recv()
             state_ref[...] = state_ref[...] * widen(
                 jnp.exp(dec_recv[d, 0:1, :])
             ) + st_recv[d].astype(f32)
@@ -559,100 +664,182 @@
             0
         ].astype(f32)
 
-    for c in late:
-        c.wait()
-
-    def project_block(b, carry):
-        at = pl.ds(pl.multiple_of(b * BLOCK, BLOCK), BLOCK)
-        y = y_ref[at, :] + jnp.dot(
+    for copy in late:
+        copy.wait()
+
+    def project_block(i, carry):
+        at = pl.ds(pl.multiple_of(i * BLOCK, BLOCK), BLOCK)
+        yy = y_ref[at, :] + jnp.dot(
             c_act[at, :], state_ref[...].astype(bf16), preferred_element_type=f32
         ) * widen(efs_ref[at, :])
-        gated = y * silu(rv_ref[at, :].astype(f32))
+        gated = yy * silu(rv_ref[at, :].astype(f32))
         gated = gated * lax.rsqrt(jnp.mean(gated * gated, axis=-1, keepdims=True) + EPSILON)
         y_norm = (gated * csv_ref[...]).astype(bf16)
         part[at, :] = jnp.dot(y_norm, mm_ref[...], preferred_element_type=f32).astype(bf16)
         return carry
 
-    lax.fori_loop(0, blocks, project_block, 0)
-
     def rows_of(t):
         return pl.ds(pl.multiple_of(t * own_rows, own_rows), own_rows)
 
-    def tp_copy(d, src, dst, send, recv):
-        return pltpu.make_async_remote_copy(
-            src_ref=src,
-            dst_ref=dst,
-            send_sem=send,
-            recv_sem=recv,
-            device_id=(me, (mt + d) % n_tp),
-            device_id_type=MESH,
-        )
-
-    first_sum = [
-        tp_copy(d, part.at[rows_of((mt + d) % n_tp)], recv1.at[d], t1_send.at[d], t1_recv.at[d])
-        for d in range(1, n_tp)
+    def near_copy(py):
+        return remote(
+            part.at[rows_of(py * 2 + 1 - c)],
+            near_recv.at[py],
+            a_send.at[py],
+            a_recv.at[py],
+            dev(z, x, y, 1 - c),
+        )
+
+    halfway = blocks // 2
+    lax.fori_loop((1 - y) * halfway, (2 - y) * halfway, project_block, 0)
+    near_copy(1 - y).start()
+    lax.fori_loop(y * halfway, (y + 1) * halfway, project_block, 0)
+    near_copy(y).start()
+
+    strips = 2
+    strip = own_rows // strips
+
+    def side_copy(k):
+        at = pl.ds(k * strip, strip)
+        return remote(
+            side_send.at[at], side_recv.at[at], b_send.at[k], b_recv.at[k], dev(z, x, 1 - y, c)
+        )
+
+    near_copy(1 - y).wait_recv()
+    for k in range(strips):
+        away = pl.ds(pl.multiple_of(((1 - y) * 2 + c) * own_rows + k * strip, strip), strip)
+        side_send[k * strip : (k + 1) * strip, :] = (
+            part[away, :].astype(f32) + near_recv[1 - y, k * strip : (k + 1) * strip, :].astype(f32)
+        ).astype(bf16)
+        side_copy(k).start()
+    near_copy(y).wait_recv()
+    relay_col(1)
+
+    def ag_copies(k):
+        lo = pl.ds(k * strip, strip)
+        to = normed.at[pl.ds(pl.multiple_of(RIM + mt * own_rows + k * strip, RIM), strip)]
+        return [
+            remote(own_norm.at[lo], to, ag_send.at[i, k], ag_recv.at[mt, k], device)
+            for i, device in enumerate((dev(mate, x, y, b), dev(z, x, 1 - y, b), dev(z, x, y, b)))
+        ]
+
+    for k in range(strips):
+        side_copy(k).wait_recv()
+        lo = slice(k * strip, (k + 1) * strip)
+        mine = pl.ds(pl.multiple_of(mt * own_rows + k * strip, strip), strip)
+        mixer = (
+            part[mine, :].astype(f32)
+            + near_recv[y, lo, :].astype(f32)
+            + side_recv[lo, :].astype(f32)
+        )
+        own_norm[lo, :] = layer_norm(
+            ALPHA * res_ref[lo, :].astype(f32) + mixer, g1_ref[...]
+        ).astype(bf16)
+        copies = ag_copies(k)
+        copies[0].start()
+        copies[1].start()
+
+        @pl.when(c != b)
+        def _(copies=copies):
+            copies[2].start()
+
+        @pl.when(c == b)
+        def _(k=k, lo=lo):
+            normed[pl.ds(pl.multiple_of(RIM + mt * own_rows + k * strip, RIM), strip), :] = own_norm[
+                lo, :
+            ]
+
+    nxt = me + 1
+    nz, nx = nxt // FAN, nxt % FAN
+    tail = jnp.logical_and(mt == n_tp - 1, nxt < n_sp)
+    halo_copies = [
+        remote(
+            own_norm.at[pl.ds(own_rows - RIM, RIM)],
+            normed.at[pl.ds(0, RIM)],
+            halo_send.at[i],
+            halo_recv,
+            dev(jnp.minimum(nz, planes - 1) // 2 * 2 + i // 2, nx, i % 2, nz % 2),
+        )
+        for i in range(4)
     ]
-    for c in first_sum:
-        c.start()
-    advance(0, 2)
-    for c in first_sum:
-        c.wait_recv()
-    mixer = part[rows_of(mt), :].astype(f32)
-    for d in range(1, n_tp):
-        mixer = mixer + recv1[d].astype(f32)
-    mine = pl.ds(pl.multiple_of(RIM + mt * own_rows, RIM), own_rows)
-    normed[mine, :] = layer_norm(
-        ALPHA * res_ref[...].astype(f32) + mixer, g1_ref[...]
-    ).astype(bf16)
-    for c in first_sum:
-        c.wait_send()
-    spread_rows = [
-        tp_copy(d, normed.at[mine], normed.at[mine], t2_send.at[d], t2_recv.at[d])
-        for d in range(1, n_tp)
-    ]
-    for c in spread_rows:
-        c.start()
-    advance(1, 2)
-    advance(0, 3)
-    for c in spread_rows:
-        c.wait()
-    rim_norm = pltpu.make_async_remote_copy(
-        src_ref=normed.at[pl.ds(rows, RIM)],
-        dst_ref=normed.at[pl.ds(0, RIM)],
-        send_sem=nr_send,
-        recv_sem=nr_recv,
-        device_id=((me + 1) % n_sp, mt),
-        device_id_type=MESH,
-    )
-
-    @pl.when(me + 1 < n_sp)
+
+    @pl.when(tail)
     def _():
-        rim_norm.start()
-
-    @pl.when(me == 0)
+        for copy in halo_copies:
+            copy.start()
+
+    send_z([3, 4, 5])
+
+    def gathered(t, k):
+        here = normed.at[pl.ds(pl.multiple_of(RIM + t * own_rows + k * strip, RIM), strip)]
+        return remote(here, here, ag_send.at[0, 0], ag_recv.at[t, k], dev(z, x, y, 1 - c))
+
+    def passed_on(pc, k):
+        here = normed.at[pl.ds(pl.multiple_of(RIM + (y * 2 + pc) * own_rows + k * strip, RIM), strip)]
+        return remote(here, here, agr_send.at[pc, k], ag_recv.at[y * 2 + pc, k], dev(z, x, 1 - y, c))
+
+    seg = (pair0 + c) * FAN + x
+    block_of = y * 2 + b
+
+    relay_x(0)
+    relay_x(1)
+    relay_col(2)
+
+    @pl.when(c != b)
+    def _():
+        for k in range(strips):
+            for pc in range(2):
+                gathered(y * 2 + pc, k).wait_recv()
+                passed_on(pc, k).start()
+
+    relay_x(2)
+    relay_col(3)
+
+    @pl.when(seg == 0)
     def _():
         normed[0:RIM, :] = jnp.zeros((RIM, width), bf16)
 
-    advance(1, 3)
-    advance(2, 1)
-    for s in range(4, half + 1):
-        advance(0, s)
-        advance(1, s)
-
-    @pl.when(me > 0)
+    @pl.when(seg > 0)
     def _():
-        rim_norm.wait_recv()
-
-    for c in own_copies:
-        c.wait()
+        halo_copies[0].wait_recv()
+
+    for k in range(strips):
+
+        @pl.when(c == b)
+        def _(k=k):
+            gathered(y * 2 + 1 - c, k).wait_recv()
+
+        for pc in range(2):
+            gathered((1 - y) * 2 + pc, k).wait_recv()
+
+    relay_x(3)
+
+    @pl.when(c == b)
+    def _():
+        for copy in own_copies:
+            copy.wait()
+
+    own_block(range(4))
+
+    def rest(who, carry):
+        @pl.when(who != me)
+        def _():
+            other_half(range(4), who)
+
+        return carry
+
+    lax.fori_loop(0, n_sp, rest, 0)
+    for copy in tap_copies:
+        copy.wait()
+    same = c == b
 
     def ffn_cols(at):
         feeds = normed[...]
         convs = []
-        for weights, taps in ((v_all, vk_ref), (w_all, wk_ref)):
+        for weights, taps, others in ((v_all, vk_ref, vk_other), (w_all, wk_ref, wk_other)):
             proj = jnp.dot(feeds, weights[:, at], preferred_element_type=f32)
             proj = proj.astype(bf16).astype(f32)
-            tap = taps[:, at].astype(f32)
+            tap = jnp.where(same, taps[:, at].astype(f32), others[:, at].astype(f32))
             total = jnp.zeros((rows, proj.shape[1]), f32)
             for k in range(FCONV):
                 start = RIM - (FCONV - 1) + k
@@ -667,9 +854,7 @@
         ffn_cols(pl.ds(pl.multiple_of(i * chunk, chunk), chunk))
         return carry
 
-    lax.fori_loop(0, full // 2, ffn_chunk, 0)
-    advance(2, 2)
-    lax.fori_loop(full // 2, full, ffn_chunk, 0)
+    lax.fori_loop(0, full, ffn_chunk, 0)
     if ff % chunk:
         ffn_cols(pl.ds(full * chunk, ff % chunk))
 
@@ -679,68 +864,135 @@
             hidden[...], s_all[who], preferred_element_type=f32
         ).astype(bf16)
 
-    def down_copies(who):
+    def down_copy(t, who):
         at = pl.ds(pl.multiple_of(who * cols, cols), cols)
-        return [
-            tp_copy(
-                d,
-                part.at[rows_of((mt + d) % n_tp), at],
-                recv2.at[d, :, at],
-                t3_send.at[d, who],
-                t3_recv.at[d, who],
-            )
-            for d in range(1, n_tp)
-        ]
-
-    down(me)
-    for c in down_copies(me):
-        c.start()
-    for k in range(1, half + 1):
-        if k >= 3:
-            advance(2, k)
-        count = 2 if k < half else 1
-
-        def both_ways(q, carry, k=k):
-            who = owner((place + n_sp - k + 2 * k * q) % n_sp)
-            down(who)
-            for c in down_copies(who):
-                c.start()
-            return carry
-
-        lax.fori_loop(0, count, both_ways, 0)
+        return remote(
+            part.at[rows_of(t), at],
+            recv2.at[block_of, :, at],
+            t3_send.at[t, who],
+            t3_recv.at[block_of, who],
+            dev(pair0 + c, x, t // 2, t % 2),
+        )
+
+    def down_step(who):
+        down(who)
+        for t in range(n_tp):
+
+            @pl.when(jnp.logical_or(c != b, mt != t))
+            def _(t=t):
+                down_copy(t, who).start()
+
+        at = pl.ds(pl.multiple_of(who * cols, cols), cols)
+
+        @pl.when(c == b)
+        def _():
+            recv2[block_of, :, at] = part[rows_of(mt), at]
+
+    near_copy(0).wait_send()
+    near_copy(1).wait_send()
+    own_block([4, 5])
+    down_step(me)
+    relay_col(4)
+    for us in ([4, 5],):
+        for u in us:
+            relay_x(u, [0])
+        other_half(us, z * FAN + 1 - x)
+    down_step(z * FAN + 1 - x)
+    relay_col(5)
+    for i in range(1, planes):
+        who = plane_at(i) * FAN + x
+        other_half([4, 5], who)
+        down_step(who)
+        relay_x(4, [i])
+    for i in range(1, planes):
+        who = plane_at(i) * FAN + 1 - x
+        relay_x(5, [i])
+        other_half([4, 5], who)
+        down_step(who)
 
     def settle(who, carry):
-        for c in down_copies(who):
-            c.wait()
+        at = pl.ds(pl.multiple_of(who * cols, cols), cols)
+        for t in range(n_tp):
+
+            @pl.when(jnp.logical_or(c != b, block_of != t))
+            def _(t=t):
+                remote(
+                    part.at[rows_of(t), at],
+                    recv2.at[t, :, at],
+                    t3_send.at[t, who],
+                    t3_recv.at[t, who],
+                    dev(z, x, y, 1 - c),
+                ).wait_recv()
+
         return carry
 
     lax.fori_loop(0, n_sp, settle, 0)
-    channel = part[rows_of(mt), :].astype(f32)
-    for d in range(1, n_tp):
-        channel = channel + recv2[d].astype(f32)
+    channel = recv2[0].astype(f32)
+    for t in range(1, n_tp):
+        channel = channel + recv2[t].astype(f32)
     out_ref[...] = layer_norm(
-        ALPHA * normed[mine, :].astype(f32) + channel, g2_ref[...]
+        ALPHA * own_norm[...].astype(f32) + channel, g2_ref[...]
     ).astype(bf16)
 
-    for piece in range(3):
-        for way in range(2):
-            for s in range(hops[piece][way]):
-                ring_copy(piece, way, s).wait_send()
-    for c in rim_copies:
-        c.wait_send()
-
-    @pl.when(me + 1 < n_sp)
+    def drain(who, carry):
+        for t in range(n_tp):
+
+            @pl.when(jnp.logical_or(c != b, mt != t))
+            def _(t=t):
+                down_copy(t, who).wait_send()
+
+        @pl.when(who != me)
+        def _():
+            for u in range(len(units)):
+                dr_copy(u, who).wait_send()
+
+        return carry
+
+    lax.fori_loop(0, n_sp, drain, 0)
+    for u in range(len(units)):
+        for i in range(1, planes):
+            xr_copy(u, i).wait_send()
+        for q in range(2):
+            for j in range(dests):
+
+                @pl.when(2 * j + c != z)
+                def _(u=u, q=q, j=j):
+                    z_copy(u, q, j).wait_send()
+
+    @pl.when(c == b)
     def _():
-        rim_norm.wait_send()
-
-    for c in state_copies(0):
-        c.wait_send()
+        for u in range(len(units)):
+            for q in range(2):
+                xo_copy(u, q).wait_send()
+                do_copy(u, q).wait_send()
+
+    for copy in rim_copies:
+        copy.wait_send()
+    for k in range(strips):
+        side_copy(k).wait_send()
+        copies = ag_copies(k)
+        copies[0].wait_send()
+        copies[1].wait_send()
+
+        @pl.when(c != b)
+        def _(k=k, copies=copies):
+            copies[2].wait_send()
+            for pc in range(2):
+                passed_on(pc, k).wait_send()
+
+    @pl.when(tail)
+    def _():
+        for copy in halo_copies:
+            copy.wait_send()
+
+    for copy in state_copies(0):
+        copy.wait_send()
     for d in range(1, half):
 
         @pl.when(me + 2 * d < n_sp)
         def _(d=d):
-            for c in state_copies(d):
-                c.wait_send()
+            for copy in state_copies(d):
+                copy.wait_send()
 
 
 def fused_shards(n_sp, n_tp, *args):
@@ -752,8 +1004,11 @@
     heads = dt.shape[1]
     width = mm.shape[1]
     ff = v.shape[1]
+    own_rows = rows // n_tp
     row = lambda a: a.reshape(1, -1)
     half = n_sp // 2
+    planes = n_sp // FAN
+    units = 3 * HALVES
     vmem = pl.BlockSpec(memory_space=pltpu.VMEM)
     hbm = pl.BlockSpec(memory_space=pl.ANY)
     dma = pltpu.SemaphoreType.DMA
@@ -769,6 +1024,8 @@
             pltpu.VMEM((RIM, inner), bf16),
             pltpu.VMEM((RIM, STATE), bf16),
             pltpu.VMEM((RIM, STATE), bf16),
+            pltpu.VMEM(vk.shape, bf16),
+            pltpu.VMEM(wk.shape, bf16),
             pltpu.VMEM((rows + RIM, 128), f32),
             pltpu.VMEM((rows, inner), bf16),
             pltpu.VMEM((rows, STATE), bf16),
@@ -786,8 +1043,11 @@
             pltpu.VMEM((half, STATE, inner), bf16),
             pltpu.VMEM((half, 8, heads), f32),
             pltpu.VMEM((rows, width), bf16),
-            pltpu.VMEM((n_tp, rows // n_tp, width), bf16),
-            pltpu.VMEM((n_tp, rows // n_tp, width), bf16),
+            pltpu.VMEM((2, own_rows, width), bf16),
+            pltpu.VMEM((own_rows, width), bf16),
+            pltpu.VMEM((own_rows, width), bf16),
+            pltpu.VMEM((own_rows, width), bf16),
+            pltpu.VMEM((n_tp, own_rows, width), bf16),
             pltpu.VMEM((rows + RIM, width), bf16),
             pltpu.VMEM((rows, ff), bf16),
             pltpu.VMEM(res.shape, bf16),
@@ -795,20 +1055,29 @@
             pltpu.VMEM(mm.shape, bf16),
             dma((3,)),
             dma((3,)),
-            dma((2, half, 3)),
-            dma((2, half, 3)),
+            dma((units, 2, n_sp)),
+            dma((units, 2, planes // 2)),
+            dma((units, 2)),
+            dma((units, 2)),
+            dma((units, planes)),
+            dma((units, n_sp)),
             dma((3,)),
             dma((3,)),
+            dma((2,)),
+            dma((2,)),
             dma((half, 2)),
             dma((half, 2)),
-            dma((n_tp,)),
-            dma((n_tp,)),
-            dma((n_tp,)),
-            dma((n_tp,)),
+            dma((2,)),
+            dma((2,)),
+            dma((2,)),
+            dma((2,)),
+            dma((3, 2)),
+            dma((n_tp, 2)),
+            dma((2, 2)),
+            dma((4,)),
+            dma,
             dma((n_tp, n_sp)),
             dma((n_tp, n_sp)),
-            dma,
-            dma,
         ],
         compiler_params=pltpu.CompilerParams(
             collective_id=0, has_side_effects=True, vmem_limit_bytes=60 * 1024 * 1024
@@ -825,11 +1094,12 @@
         fits = (
             args[3].shape[1] == STATE
             and args[18].shape[1] % 128 == 0
-            and args[16].shape[0] % 16 == 0
+            and args[16].shape[0] % 64 == 0
             and args[16].shape[1] % 128 == 0
-            and n_sp % 2 == 0
-            and n_sp >= 4
-            and args[18].shape[0] % 32 == 0
+            and n_sp % (2 * FAN) == 0
+            and n_sp > 2 * FAN
+            and n_tp == 4
+            and args[18].shape[0] % 64 == 0
             and rows % (BLOCK * n_tp) == 0
         )
         if fits:

time: 193 us -> 161 us (0.83)
  Pallas kernels: 191 us -> 158 us
    pallas_call x1, Pallas kernels: 191 us -> 158 us  [fused_shards(): pl.pallas_call(functools.partial(layer_kernel, n_sp, n_tp), out_shape=jax...]
where the time goes in v1:
time: 161 us; the launch traced here: 160 us
  Pallas kernels  158 us (98%)
  local copies, waits for them, and re-layouts  1.88 us (1%)
    pallas_call x1, Pallas kernels, fused_shards(): pl.pallas_call(functools.partial(layer_kernel, n_sp, n_tp), out_shape=jax...  158 us

profile of v1, /device:TPU:19, one launch (start us, length us, event | category | flops | bytes accessed | tf_op | source)
XLA Modules:
  0.0 160.3 jit_solution(14137691254092852517)
XLA Ops:
  0.0 158.4 %shard_map.208 = bf16[128,2048]{1,0:T(8,128)(2,1)} custom-call(bf16[128,2048]{1,0:T(8,128)(2,1)} %res_hbm.1, bf16[512,512]{1,0:T(8,128)(2,1)} %rv_hbm.1, bf16[512,512]{1,0:T(8,128)(2,1)} %xf_ref.1, bf16[512,128]{1,0:T(8,128)(2,1)} %bf_ref.1, bf16[512,128]{1,0:T(8,128)(2,1)} %cf_ref.1, f32[8,512]{1,0:T(8,128)} %bitcast.8, f32[1,8]{1,0:T(1,128)} %bitcast.13, ...), custom_call_target="tpu_custom_call" | custom-call | tf_op jit(solution)/shard_map/pallas_call | solution.py:1015
  158.4 1.9 %copy.24 = bf16[128,2048]{1,0:T(8,128)(2,1)} copy(bf16[128,2048]{1,0:T(8,128)(2,1)} %shard_map.208) | data formatting | bytes 1048576

commit v2 on v1

--- a/solution.py
+++ b/solution.py
@@ -225,7 +225,7 @@
 MESH = pl.DeviceIdType.MESH
 RIM = 16
 FAN = 2
-HALVES = 2
+CUTS = (2, 2, 4)
 
 
 def silu(v):
@@ -288,6 +288,7 @@
     side_recv,
     own_norm,
     recv2,
+    pre_recv,
     normed,
     hidden,
     res_ref,
@@ -318,6 +319,8 @@
     halo_recv,
     t3_send,
     t3_recv,
+    p_send,
+    p_recv,
 ):
     f32, bf16 = jnp.float32, jnp.bfloat16
     rows, inner = xf_ref.shape
@@ -355,13 +358,13 @@
         pl.semaphore_signal(barrier, inc=1, device_id=(who // n_tp, who % n_tp), device_id_type=MESH)
     pl.semaphore_wait(barrier, total_devices - 1)
 
-    units = [(kind, g) for kind in range(3) for g in range(HALVES)]
+    units = [(kind, g) for kind in range(3) for g in range(CUTS[kind])]
     sources = (v_hbm, w_hbm, s_hbm)
 
     def place(u, q):
         kind, g = units[u]
-        size = (ff if kind == 2 else depth) // (2 * HALVES)
-        return size, (q * HALVES + g) * size
+        size = (ff if kind == 2 else depth) // (2 * CUTS[kind])
+        return size, (q * CUTS[kind] + g) * size
 
     def own_piece(u, q):
         size, at = place(u, q)
@@ -419,14 +422,22 @@
         got = jnp.where(i - 1 < low, i - 1, i)
         return jnp.where(z < planes // 2, got, planes - 1 - got)
 
-    def send_z(which):
-        for u in which:
-            for q in range(2):
-                for j in range(dests):
-
-                    @pl.when(2 * j + c != z)
-                    def _(u=u, q=q, j=j):
-                        z_copy(u, q, j).start()
+    def send_z(pieces, only=True):
+        for u, q in pieces:
+            for j in range(dests):
+
+                @pl.when(jnp.logical_and(2 * j + c != z, only if only is True else only(2 * j + c)))
+                def _(u=u, q=q, j=j):
+                    z_copy(u, q, j).start()
+
+    def both(us):
+        return [(u, q) for u in us for q in range(2)]
+
+    def held(to):
+        return jnp.logical_and(jnp.logical_and(b == 0, to > z), z < planes - 2)
+
+    def free(to):
+        return jnp.logical_not(held(to))
 
     def send_xo(which):
         @pl.when(c == b)
@@ -477,8 +488,8 @@
     ]
     for copy in tap_copies:
         copy.start()
-    send_z([0])
-    send_xo([0, 1, 2, 3])
+    send_z(both([0]))
+    send_xo([0, 1])
 
     own_copies = []
     for kind in range(3):
@@ -610,59 +621,80 @@
     odd = me % 2
     partner = me + 1 - 2 * odd
 
-    def state_copies(d):
-        pair = d > 0
+    pairs = planes // 2
+    own_pair = z // 2
+
+    def state_copy(src, src_dec, at, sent, device):
         return [
-            remote(
-                src,
-                dst.at[d],
-                st_ssem.at[d, i],
-                st_rsem.at[d, i],
-                ((me + 2 * d) % n_sp if pair else partner, mt),
-            )
-            for i, (src, dst) in enumerate(
-                ((pair_send if pair else st_send, st_recv), (pair_dec if pair else dec_send, dec_recv))
-            )
+            remote(a, o.at[at], st_ssem.at[sent, i], st_rsem.at[at, i], device)
+            for i, (a, o) in enumerate(((src, st_recv), (src_dec, dec_recv)))
         ]
 
-    for copy in state_copies(0):
+    beside_copies = state_copy(st_send, dec_send, 0, 0, (partner, mt))
+    mate_copies = state_copy(pair_send, pair_dec, 1, 1, dev(mate, x, y, c))
+
+    def quad_copies(j, side):
+        to = jnp.minimum(2 * j + side, planes - 1)
+        return state_copy(pair_send, pair_dec, 2 + own_pair, 2 + 2 * j + side, dev(to, x, y, c))
+
+    for copy in beside_copies:
         copy.start()
-    send_xo([4, 5])
-    for copy in state_copies(0):
+    for copy in beside_copies:
         copy.wait_recv()
     own_dec = widen(jnp.exp(dec_send[0:1, :]))
     beside_dec = widen(jnp.exp(dec_recv[0, 0:1, :]))
     beside = st_recv[0].astype(f32)
     later = odd == 1
-    pair_send[...] = jnp.where(
+    plane_state = jnp.where(
         later, state_ref[...] + beside * own_dec, state_ref[...] * beside_dec + beside
-    ).astype(bf16)
-    pair_dec[...] = dec_send[...] + dec_recv[0]
+    )
+
+    @pl.when(b == 0)
+    def _():
+        pair_send[...] = plane_state.astype(bf16)
+        pair_dec[...] = dec_send[...] + dec_recv[0]
+        for copy in mate_copies:
+            copy.start()
+
+    @pl.when(b == 1)
+    def _():
+        for copy in mate_copies:
+            copy.wait_recv()
+        plane_dec = dec_send[...] + dec_recv[0]
+        pair_send[...] = (
+            st_recv[1].astype(f32) * widen(jnp.exp(plane_dec[0:1, :])) + plane_state
+        ).astype(bf16)
+        pair_dec[...] = plane_dec + dec_recv[1]
+        for j in range(1, pairs):
+            for side in (1, 0):
+
+                @pl.when(own_pair < j)
+                def _(j=j, side=side):
+                    for copy in quad_copies(j, side):
+                        copy.start()
+
     state_ref[...] = jnp.zeros_like(state_ref)
-    for d in range(1, half):
-
-        @pl.when(me + 2 * d < n_sp)
-        def _(d=d):
-            for copy in state_copies(d):
-                copy.start()
-
-    send_z([1, 2])
-    relay_col(0)
-    for d in range(half - 1, 0, -1):
-
-        @pl.when(me >= 2 * d)
-        def _(d=d):
-            for copy in state_copies(d):
+    send_z(both([1, 2]), free)
+    send_xo(range(2, len(units)))
+
+    def join(at):
+        state_ref[...] = state_ref[...] * widen(jnp.exp(dec_recv[at, 0:1, :])) + st_recv[at].astype(f32)
+
+    for j in range(pairs - 1):
+
+        @pl.when(own_pair > j)
+        def _(j=j):
+            for copy in state_copy(pair_send, pair_dec, 2 + j, 0, dev(mate, x, y, c)):
                 copy.wait_recv()
-            state_ref[...] = state_ref[...] * widen(
-                jnp.exp(dec_recv[d, 0:1, :])
-            ) + st_recv[d].astype(f32)
+            join(2 + j)
+
+    @pl.when(b == 1)
+    def _():
+        join(1)
 
     @pl.when(odd == 1)
     def _():
-        state_ref[...] = state_ref[...] * widen(jnp.exp(dec_recv[0, 0:1, :])) + st_recv[
-            0
-        ].astype(f32)
+        join(0)
 
     for copy in late:
         copy.wait()
@@ -713,7 +745,7 @@
         ).astype(bf16)
         side_copy(k).start()
     near_copy(y).wait_recv()
-    relay_col(1)
+    relay_col(0)
 
     def ag_copies(k):
         lo = pl.ds(k * strip, strip)
@@ -768,7 +800,15 @@
         for copy in halo_copies:
             copy.start()
 
-    send_z([3, 4, 5])
+    send_z(both([1, 2]), held)
+    send_z(both([3]))
+    outer = jnp.logical_or(z == 0, z == planes - 1)
+    shrink = range(4, len(units))
+
+    def far_outer(to):
+        return jnp.logical_and(outer, jnp.abs(to - z) > 1)
+
+    send_z(both(shrink), lambda to: jnp.logical_not(far_outer(to)))
 
     def gathered(t, k):
         here = normed.at[pl.ds(pl.multiple_of(RIM + t * own_rows + k * strip, RIM), strip)]
@@ -779,11 +819,8 @@
         return remote(here, here, agr_send.at[pc, k], ag_recv.at[y * 2 + pc, k], dev(z, x, 1 - y, c))
 
     seg = (pair0 + c) * FAN + x
-    block_of = y * 2 + b
-
-    relay_x(0)
-    relay_x(1)
-    relay_col(2)
+
+    relay_col(1)
 
     @pl.when(c != b)
     def _():
@@ -792,9 +829,8 @@
                 gathered(y * 2 + pc, k).wait_recv()
                 passed_on(pc, k).start()
 
-    relay_x(2)
+    relay_col(2)
     relay_col(3)
-
     @pl.when(seg == 0)
     def _():
         normed[0:RIM, :] = jnp.zeros((RIM, width), bf16)
@@ -812,7 +848,8 @@
         for pc in range(2):
             gathered((1 - y) * 2 + pc, k).wait_recv()
 
-    relay_x(3)
+    for u in range(4):
+        relay_x(u)
 
     @pl.when(c == b)
     def _():
@@ -831,6 +868,7 @@
     lax.fori_loop(0, n_sp, rest, 0)
     for copy in tap_copies:
         copy.wait()
+    send_z(both(shrink), lambda to: jnp.logical_and(far_outer(to), to < z))
     same = c == b
 
     def ffn_cols(at):
@@ -854,7 +892,16 @@
         ffn_cols(pl.ds(pl.multiple_of(i * chunk, chunk), chunk))
         return carry
 
-    lax.fori_loop(0, full, ffn_chunk, 0)
+    def relay_s(i):
+        for u in shrink:
+            relay_col(u, [i])
+
+    relay_s(1)
+    lax.fori_loop(0, full // 2, ffn_chunk, 0)
+    relay_s(2)
+    lax.fori_loop(full // 2, full // 2 + 1, ffn_chunk, 0)
+    send_z(both(shrink), lambda to: jnp.logical_and(far_outer(to), to > z))
+    lax.fori_loop(full // 2 + 1, full, ffn_chunk, 0)
     if ff % chunk:
         ffn_cols(pl.ds(full * chunk, ff % chunk))
 
@@ -864,57 +911,111 @@
             hidden[...], s_all[who], preferred_element_type=f32
         ).astype(bf16)
 
-    def down_copy(t, who):
-        at = pl.ds(pl.multiple_of(who * cols, cols), cols)
+    def at_of(who):
+        return pl.ds(pl.multiple_of(who * cols, cols), cols)
+
+    def side_half(py):
+        return pl.ds(pl.multiple_of(py * 2 * own_rows, own_rows), 2 * own_rows)
+
+    def home_copies(who):
+        at = at_of(who)
+        return [
+            remote(
+                part.at[rows_of(py * 2 + pc), at],
+                recv2.at[y, :, at],
+                t3_send.at[i, who],
+                t3_recv.at[y, who],
+                dev(z, x, py, pc),
+            )
+            for i, (py, pc) in enumerate(((1 - y, 0), (1 - y, 1), (y, 1 - c)))
+        ]
+
+    def cross_copy(who):
+        at = at_of(who)
         return remote(
-            part.at[rows_of(t), at],
-            recv2.at[block_of, :, at],
-            t3_send.at[t, who],
-            t3_recv.at[block_of, who],
-            dev(pair0 + c, x, t // 2, t % 2),
-        )
+            part.at[side_half(1 - y), at], pre_recv.at[:, at], p_send.at[who], p_recv.at[who], dev(z, x, 1 - y, c)
+        )
+
+    def away_copies(who):
+        at = at_of(who)
+        return [
+            remote(
+                part.at[rows_of(y * 2 + pc), at],
+                recv2.at[2, :, at],
+                t3_send.at[pc, who],
+                t3_recv.at[2, who],
+                dev(mate, x, y, pc),
+            )
+            for pc in range(2)
+        ]
+
+    done = []
+    lag = 2
+
+    def finish(who):
+        at = at_of(who)
+
+        @pl.when(c != b)
+        def _():
+            cross_copy(who).wait_recv()
+            here = side_half(y)
+            part[here, at] = (part[here, at].astype(f32) + pre_recv[:, at].astype(f32)).astype(bf16)
+            for copy in away_copies(who):
+                copy.start()
 
     def down_step(who):
         down(who)
-        for t in range(n_tp):
-
-            @pl.when(jnp.logical_or(c != b, mt != t))
-            def _(t=t):
-                down_copy(t, who).start()
-
-        at = pl.ds(pl.multiple_of(who * cols, cols), cols)
+        at = at_of(who)
+
+        @pl.when(c != b)
+        def _():
+            cross_copy(who).start()
 
         @pl.when(c == b)
         def _():
-            recv2[block_of, :, at] = part[rows_of(mt), at]
+            for copy in home_copies(who):
+                copy.start()
+            recv2[y, :, at] = part[rows_of(mt), at]
+
+        done.append(who)
+        if len(done) > lag:
+            finish(done[-1 - lag])
 
     near_copy(0).wait_send()
     near_copy(1).wait_send()
-    own_block([4, 5])
+    own_block(shrink)
     down_step(me)
-    relay_col(4)
-    for us in ([4, 5],):
-        for u in us:
-            relay_x(u, [0])
-        other_half(us, z * FAN + 1 - x)
-    down_step(z * FAN + 1 - x)
-    relay_col(5)
-    for i in range(1, planes):
+
+    def x_step(i):
+        who = plane_at(i) * FAN + 1 - x
+        for u in shrink:
+            relay_x(u, [i])
+        other_half(shrink, who)
+        down_step(who)
+
+    def col_step(i):
         who = plane_at(i) * FAN + x
-        other_half([4, 5], who)
+        other_half(shrink, who)
         down_step(who)
-        relay_x(4, [i])
-    for i in range(1, planes):
-        who = plane_at(i) * FAN + 1 - x
-        relay_x(5, [i])
-        other_half([4, 5], who)
-        down_step(who)
+
+    x_step(0)
+    col_step(1)
+    x_step(1)
+    for i in range(2, planes - 1):
+        col_step(i)
+        for u in shrink:
+            relay_col(u, [i + 1])
+        x_step(i)
+    col_step(planes - 1)
+    x_step(planes - 1)
+    for who in done[-lag:]:
+        finish(who)
 
     def settle(who, carry):
-        at = pl.ds(pl.multiple_of(who * cols, cols), cols)
-        for t in range(n_tp):
-
-            @pl.when(jnp.logical_or(c != b, block_of != t))
+        at = at_of(who)
+        for t in range(3):
+
+            @pl.when(jnp.logical_or(c != b, y != t))
             def _(t=t):
                 remote(
                     part.at[rows_of(t), at],
@@ -928,18 +1029,23 @@
 
     lax.fori_loop(0, n_sp, settle, 0)
     channel = recv2[0].astype(f32)
-    for t in range(1, n_tp):
+    for t in range(1, 3):
         channel = channel + recv2[t].astype(f32)
     out_ref[...] = layer_norm(
         ALPHA * own_norm[...].astype(f32) + channel, g2_ref[...]
     ).astype(bf16)
 
     def drain(who, carry):
-        for t in range(n_tp):
-
-            @pl.when(jnp.logical_or(c != b, mt != t))
-            def _(t=t):
-                down_copy(t, who).wait_send()
+        @pl.when(c == b)
+        def _():
+            for copy in home_copies(who):
+                copy.wait_send()
+
+        @pl.when(c != b)
+        def _():
+            cross_copy(who).wait_send()
+            for copy in away_copies(who):
+                copy.wait_send()
 
         @pl.when(who != me)
         def _():
@@ -985,14 +1091,21 @@
         for copy in halo_copies:
             copy.wait_send()
 
-    for copy in state_copies(0):
+    for copy in beside_copies:
         copy.wait_send()
-    for d in range(1, half):
-
-        @pl.when(me + 2 * d < n_sp)
-        def _(d=d):
-            for copy in state_copies(d):
-                copy.wait_send()
+
+    @pl.when(b == 0)
+    def _():
+        for copy in mate_copies:
+            copy.wait_send()
+
+    for j in range(1, pairs):
+        for side in range(2):
+
+            @pl.when(jnp.logical_and(b == 1, own_pair < j))
+            def _(j=j, side=side):
+                for copy in quad_copies(j, side):
+                    copy.wait_send()
 
 
 def fused_shards(n_sp, n_tp, *args):
@@ -1008,7 +1121,7 @@
     row = lambda a: a.reshape(1, -1)
     half = n_sp // 2
     planes = n_sp // FAN
-    units = 3 * HALVES
+    units = sum(CUTS)
     vmem = pl.BlockSpec(memory_space=pltpu.VMEM)
     hbm = pl.BlockSpec(memory_space=pl.ANY)
     dma = pltpu.SemaphoreType.DMA
@@ -1047,7 +1160,8 @@
             pltpu.VMEM((own_rows, width), bf16),
             pltpu.VMEM((own_rows, width), bf16),
             pltpu.VMEM((own_rows, width), bf16),
-            pltpu.VMEM((n_tp, own_rows, width), bf16),
+            pltpu.VMEM((3, own_rows, width), bf16),
+            pltpu.VMEM((2 * own_rows, width), bf16),
             pltpu.VMEM((rows + RIM, width), bf16),
             pltpu.VMEM((rows, ff), bf16),
             pltpu.VMEM(res.shape, bf16),
@@ -1065,7 +1179,7 @@
             dma((3,)),
             dma((2,)),
             dma((2,)),
-            dma((half, 2)),
+            dma((2 + planes, 2)),
             dma((half, 2)),
             dma((2,)),
             dma((2,)),
@@ -1076,8 +1190,10 @@
             dma((2, 2)),
             dma((4,)),
             dma,
-            dma((n_tp, n_sp)),
-            dma((n_tp, n_sp)),
+            dma((3, n_sp)),
+            dma((3, n_sp)),
+            dma((n_sp,)),
+            dma((n_sp,)),
         ],
         compiler_params=pltpu.CompilerParams(
             collective_id=0, has_side_effects=True, vmem_limit_bytes=60 * 1024 * 1024

time: 161 us -> 140 us (0.87)
  Pallas kernels: 158 us -> 138 us
    pallas_call x1, Pallas kernels: 158 us -> 138 us  [fused_shards(): pl.pallas_call(functools.partial(layer_kernel, n_sp, n_tp), out_shape=jax...]
where the time goes in v2:
time: 140 us
  Pallas kernels  138 us (99%)
  local copies, waits for them, and re-layouts  1.88 us (1%)
    pallas_call x1, Pallas kernels, fused_shards(): pl.pallas_call(functools.partial(layer_kernel, n_sp, n_tp), out_shape=jax...  138 us

profile of v2, /device:TPU:19, one launch (start us, length us, event | category | flops | bytes accessed | tf_op | source)
XLA Modules:
  0.0 139.6 jit_solution(17916469887224548724)
XLA Ops:
  0.0 137.7 %shard_map.208 = bf16[128,2048]{1,0:T(8,128)(2,1)} custom-call(bf16[128,2048]{1,0:T(8,128)(2,1)} %res_hbm.1, bf16[512,512]{1,0:T(8,128)(2,1)} %rv_hbm.1, bf16[512,512]{1,0:T(8,128)(2,1)} %xf_ref.1, bf16[512,128]{1,0:T(8,128)(2,1)} %bf_ref.1, bf16[512,128]{1,0:T(8,128)(2,1)} %cf_ref.1, f32[8,512]{1,0:T(8,128)} %bitcast.8, f32[1,8]{1,0:T(1,128)} %bitcast.13, ...), custom_call_target="tpu_custom_call" | custom-call | tf_op jit(solution)/shard_map/pallas_call | solution.py:1128
  137.7 1.9 %copy.24 = bf16[128,2048]{1,0:T(8,128)(2,1)} copy(bf16[128,2048]{1,0:T(8,128)(2,1)} %shard_map.208) | data formatting | bytes 1048576

commit v3 on v2

--- a/solution.py
+++ b/solution.py
@@ -290,13 +290,18 @@
     recv2,
     pre_recv,
     normed,
+    gate_act,
     hidden,
     res_ref,
     rv_ref,
     mm_ref,
     late_sem,
     own_sem,
-    w_recv,
+    col_recv,
+    xvw_recv,
+    xs_recv,
+    dv_recv,
+    ds_recv,
     z_send,
     xo_send,
     do_send,
@@ -378,42 +383,41 @@
         whole = v_all if kind == 0 else w_all
         return whole.at[pl.ds(pl.multiple_of(who * depth + at, 16), size)]
 
-    def landed(u, q, who):
-        here = slot(u, q, who)
-        return remote(here, here, do_send.at[0, 0], w_recv.at[u, q, who], dev(z, x, y, 1 - c))
+    wide = [u for u, (kind, g) in enumerate(units) if kind < 2]
+    shrink = [u for u, (kind, g) in enumerate(units) if kind == 2]
+
+    def x_sem(u, pz):
+        return xvw_recv.at[u] if u in wide else xs_recv.at[pz]
+
+    def d_sem(u, who):
+        return dv_recv.at[units[u][0]] if u in wide else ds_recv.at[who]
+
+    def arrived(sem, count):
+        here = v_all.at[pl.ds(0, count)]
+        remote(here, here, do_send, sem, dev(z, x, y, 1 - c)).wait_recv()
+
+    def left(sem, count):
+        here = v_all.at[pl.ds(0, count)]
+        remote(here, here, sem, dv_recv.at[0], dev(z, x, y, 1 - c)).wait_send()
 
     def z_copy(u, q, j):
         return remote(
-            own_piece(u, q),
-            slot(u, q, me),
-            z_send.at[u, q, j],
-            w_recv.at[u, q, me],
-            dev(2 * j + c, x, y, q),
+            own_piece(u, q), slot(u, q, me), z_send.at[j], col_recv.at[u, z], dev(2 * j + c, x, y, q)
         )
 
     def xo_copy(u, q):
-        return remote(
-            own_piece(u, q), slot(u, q, me), xo_send.at[u, q], w_recv.at[u, q, me], dev(z, 1 - x, y, q)
-        )
+        return remote(own_piece(u, q), slot(u, q, me), xo_send, x_sem(u, z), dev(z, 1 - x, y, q))
 
     def do_copy(u, q):
-        return remote(
-            own_piece(u, q), slot(u, q, me), do_send.at[u, q], w_recv.at[u, q, me], dev(z, x, y, 1 - c)
-        )
+        return remote(own_piece(u, q), slot(u, q, me), do_send, d_sem(u, me), dev(z, x, y, 1 - c))
 
     def xr_copy(u, i):
         here = slot(u, c, plane_at(i) * FAN + x)
-        return remote(
-            here,
-            here,
-            xr_send.at[u, i],
-            w_recv.at[u, c, plane_at(i) * FAN + x],
-            dev(z, 1 - x, y, c),
-        )
-
-    def dr_copy(u, who):
+        return remote(here, here, xr_send, x_sem(u, plane_at(i)), dev(z, 1 - x, y, c))
+
+    def dr_copy(u, who, side):
         here = slot(u, c, who)
-        return remote(here, here, dr_send.at[u, who], w_recv.at[u, c, who], dev(z, x, y, 1 - c))
+        return remote(here, here, dr_send.at[side], d_sem(u, who), dev(z, x, y, 1 - c))
 
     def plane_at(i):
         if i == 0:
@@ -434,7 +438,7 @@
         return [(u, q) for u in us for q in range(2)]
 
     def held(to):
-        return jnp.logical_and(jnp.logical_and(b == 0, to > z), z < planes - 2)
+        return jnp.logical_and(jnp.logical_and(b == 0, to > z + 1), z < planes - 2)
 
     def free(to):
         return jnp.logical_not(held(to))
@@ -449,26 +453,33 @@
     def relay_col(u, picks=None):
         for i in picks or range(1, planes):
             who = plane_at(i) * FAN + x
-            landed(u, c, who).wait_recv()
+            here = slot(u, c, who)
+            remote(
+                here, here, do_send, col_recv.at[u, plane_at(i)], dev(z, x, y, 1 - c)
+            ).wait_recv()
             xr_copy(u, i).start()
-            dr_copy(u, who).start()
-
-    def relay_x(u, picks=None):
-        for i in picks or range(planes):
-            who = plane_at(i) * FAN + 1 - x
-            landed(u, c, who).wait_recv()
-            dr_copy(u, who).start()
-
-    def other_half(us, who):
-        for u in us:
-            landed(u, 1 - c, who).wait_recv()
-
-    def own_block(us):
+            dr_copy(u, who, 0).start()
+
+    def relay_x(u):
+        arrived(xvw_recv.at[u], planes * place(u, 0)[0])
+        for i in range(planes):
+            dr_copy(u, plane_at(i) * FAN + 1 - x, 1).start()
+
+    def relay_xs(i):
+        arrived(xs_recv.at[plane_at(i)], depth // 2)
+        for u in shrink:
+            dr_copy(u, plane_at(i) * FAN + 1 - x, 1).start()
+
+    def complete(kind):
+        rest = (n_sp - 1) * depth // 2
+
+        @pl.when(c == b)
+        def _():
+            arrived(dv_recv.at[kind], rest)
+
         @pl.when(c != b)
         def _():
-            for u in us:
-                for q in range(2):
-                    landed(u, q, me).wait_recv()
+            arrived(dv_recv.at[kind], rest + depth)
 
     rim_copies = []
     for i, (src, dst) in enumerate(((xf_ref, rim_x), (bf_ref, rim_b), (cf_ref, rim_c))):
@@ -803,8 +814,6 @@
     send_z(both([1, 2]), held)
     send_z(both([3]))
     outer = jnp.logical_or(z == 0, z == planes - 1)
-    shrink = range(4, len(units))
-
     def far_outer(to):
         return jnp.logical_and(outer, jnp.abs(to - z) > 1)
 
@@ -848,7 +857,7 @@
         for pc in range(2):
             gathered((1 - y) * 2 + pc, k).wait_recv()
 
-    for u in range(4):
+    for u in range(3):
         relay_x(u)
 
     @pl.when(c == b)
@@ -856,54 +865,57 @@
         for copy in own_copies:
             copy.wait()
 
-    own_block(range(4))
-
-    def rest(who, carry):
-        @pl.when(who != me)
-        def _():
-            other_half(range(4), who)
-
-        return carry
-
-    lax.fori_loop(0, n_sp, rest, 0)
     for copy in tap_copies:
         copy.wait()
-    send_z(both(shrink), lambda to: jnp.logical_and(far_outer(to), to < z))
     same = c == b
 
-    def ffn_cols(at):
-        feeds = normed[...]
-        convs = []
-        for weights, taps, others in ((v_all, vk_ref, vk_other), (w_all, wk_ref, wk_other)):
-            proj = jnp.dot(feeds, weights[:, at], preferred_element_type=f32)
-            proj = proj.astype(bf16).astype(f32)
-            tap = jnp.where(same, taps[:, at].astype(f32), others[:, at].astype(f32))
-            total = jnp.zeros((rows, proj.shape[1]), f32)
-            for k in range(FCONV):
-                start = RIM - (FCONV - 1) + k
-                total = total + tap[k : k + 1] * proj[start : start + rows, :]
-            convs.append(total)
-        hidden[:, at] = (silu(convs[0]) * convs[1]).astype(bf16)
+    def conv_cols(at, weights, taps, others):
+        proj = jnp.dot(normed[...], weights[:, at], preferred_element_type=f32)
+        proj = proj.astype(bf16).astype(f32)
+        tap = jnp.where(same, taps[:, at].astype(f32), others[:, at].astype(f32))
+        total = jnp.zeros((rows, proj.shape[1]), f32)
+        for k in range(FCONV):
+            start = RIM - (FCONV - 1) + k
+            total = total + tap[k : k + 1] * proj[start : start + rows, :]
+        return total
+
+    def gate_cols(at):
+        gate_act[:, at] = silu(conv_cols(at, v_all, vk_ref, vk_other))
+
+    def up_cols(at):
+        hidden[:, at] = (gate_act[:, at] * conv_cols(at, w_all, wk_ref, wk_other)).astype(bf16)
 
     chunk = 256
     full = ff // chunk
 
-    def ffn_chunk(i, carry):
-        ffn_cols(pl.ds(pl.multiple_of(i * chunk, chunk), chunk))
-        return carry
+    def run_cols(fn, lo, hi):
+        def one(i, carry):
+            fn(pl.ds(pl.multiple_of(i * chunk, chunk), chunk))
+            return carry
+
+        lax.fori_loop(lo, hi, one, 0)
+
+    def rest_cols(fn):
+        if ff % chunk:
+            fn(pl.ds(full * chunk, ff % chunk))
+
+    complete(0)
+    run_cols(gate_cols, 0, full)
+    rest_cols(gate_cols)
+    send_z(both(shrink), lambda to: jnp.logical_and(far_outer(to), to < z))
+    relay_x(3)
+    complete(1)
 
     def relay_s(i):
         for u in shrink:
             relay_col(u, [i])
 
     relay_s(1)
-    lax.fori_loop(0, full // 2, ffn_chunk, 0)
+    run_cols(up_cols, 0, full // 2)
     relay_s(2)
-    lax.fori_loop(full // 2, full // 2 + 1, ffn_chunk, 0)
+    run_cols(up_cols, full // 2, full)
+    rest_cols(up_cols)
     send_z(both(shrink), lambda to: jnp.logical_and(far_outer(to), to > z))
-    lax.fori_loop(full // 2 + 1, full, ffn_chunk, 0)
-    if ff % chunk:
-        ffn_cols(pl.ds(full * chunk, ff % chunk))
 
     def down(who):
         at = pl.ds(pl.multiple_of(who * cols, cols), cols)
@@ -923,17 +935,17 @@
             remote(
                 part.at[rows_of(py * 2 + pc), at],
                 recv2.at[y, :, at],
-                t3_send.at[i, who],
-                t3_recv.at[y, who],
+                t3_send,
+                t3_recv.at[y],
                 dev(z, x, py, pc),
             )
-            for i, (py, pc) in enumerate(((1 - y, 0), (1 - y, 1), (y, 1 - c)))
+            for py, pc in ((1 - y, 0), (1 - y, 1), (y, 1 - c))
         ]
 
     def cross_copy(who):
         at = at_of(who)
         return remote(
-            part.at[side_half(1 - y), at], pre_recv.at[:, at], p_send.at[who], p_recv.at[who], dev(z, x, 1 - y, c)
+            part.at[side_half(1 - y), at], pre_recv.at[:, at], p_send, p_recv.at[who], dev(z, x, 1 - y, c)
         )
 
     def away_copies(who):
@@ -942,8 +954,8 @@
             remote(
                 part.at[rows_of(y * 2 + pc), at],
                 recv2.at[2, :, at],
-                t3_send.at[pc, who],
-                t3_recv.at[2, who],
+                t3_send,
+                t3_recv.at[2],
                 dev(mate, x, y, pc),
             )
             for pc in range(2)
@@ -983,51 +995,47 @@
 
     near_copy(0).wait_send()
     near_copy(1).wait_send()
-    own_block(shrink)
+
+    @pl.when(c != b)
+    def _():
+        arrived(ds_recv.at[me], depth)
+
     down_step(me)
 
     def x_step(i):
         who = plane_at(i) * FAN + 1 - x
-        for u in shrink:
-            relay_x(u, [i])
-        other_half(shrink, who)
+        relay_xs(i)
+        arrived(ds_recv.at[who], depth // 2)
         down_step(who)
 
     def col_step(i):
         who = plane_at(i) * FAN + x
-        other_half(shrink, who)
+        arrived(ds_recv.at[who], depth // 2)
         down_step(who)
 
     x_step(0)
     col_step(1)
+    last = planes - 1
+    relay_col(4, [last])
+    relay_col(5, [last])
     x_step(1)
-    for i in range(2, planes - 1):
+    relay_col(6, [last])
+    for i in range(2, last):
         col_step(i)
-        for u in shrink:
-            relay_col(u, [i + 1])
+        if i == 2:
+            relay_col(7, [last])
         x_step(i)
-    col_step(planes - 1)
-    x_step(planes - 1)
+    col_step(last)
+    x_step(last)
     for who in done[-lag:]:
         finish(who)
 
-    def settle(who, carry):
-        at = at_of(who)
-        for t in range(3):
-
-            @pl.when(jnp.logical_or(c != b, y != t))
-            def _(t=t):
-                remote(
-                    part.at[rows_of(t), at],
-                    recv2.at[t, :, at],
-                    t3_send.at[t, who],
-                    t3_recv.at[t, who],
-                    dev(z, x, y, 1 - c),
-                ).wait_recv()
-
-        return carry
-
-    lax.fori_loop(0, n_sp, settle, 0)
+    for t in range(3):
+
+        @pl.when(jnp.logical_or(c != b, y != t))
+        def _(t=t):
+            remote(recv2.at[t], recv2.at[t], t3_send, t3_recv.at[t], dev(z, x, y, 1 - c)).wait_recv()
+
     channel = recv2[0].astype(f32)
     for t in range(1, 3):
         channel = channel + recv2[t].astype(f32)
@@ -1035,42 +1043,30 @@
         ALPHA * own_norm[...].astype(f32) + channel, g2_ref[...]
     ).astype(bf16)
 
-    def drain(who, carry):
-        @pl.when(c == b)
-        def _():
-            for copy in home_copies(who):
-                copy.wait_send()
-
-        @pl.when(c != b)
-        def _():
-            cross_copy(who).wait_send()
-            for copy in away_copies(who):
-                copy.wait_send()
-
-        @pl.when(who != me)
-        def _():
-            for u in range(len(units)):
-                dr_copy(u, who).wait_send()
-
-        return carry
-
-    lax.fori_loop(0, n_sp, drain, 0)
-    for u in range(len(units)):
-        for i in range(1, planes):
-            xr_copy(u, i).wait_send()
-        for q in range(2):
-            for j in range(dests):
-
-                @pl.when(2 * j + c != z)
-                def _(u=u, q=q, j=j):
-                    z_copy(u, q, j).wait_send()
+    def part_left(sem, count):
+        here = part.at[pl.ds(0, count)]
+        remote(here, here, sem, t3_recv.at[0], dev(z, x, y, 1 - c)).wait_send()
 
     @pl.when(c == b)
     def _():
-        for u in range(len(units)):
-            for q in range(2):
-                xo_copy(u, q).wait_send()
-                do_copy(u, q).wait_send()
+        part_left(t3_send, 3 * own_rows)
+        left(xo_send, 3 * depth)
+        left(do_send, 3 * depth)
+
+    @pl.when(c != b)
+    def _():
+        part_left(t3_send, 2 * own_rows)
+        part_left(p_send, 2 * own_rows)
+
+    half_blocks = 3 * depth // 2
+    left(xr_send, (planes - 1) * half_blocks)
+    left(dr_send.at[0], (planes - 1) * half_blocks)
+    left(dr_send.at[1], planes * half_blocks)
+    for j in range(dests):
+
+        @pl.when(2 * j + c != z)
+        def _(j=j):
+            left(z_send.at[j], 3 * depth)
 
     for copy in rim_copies:
         copy.wait_send()
@@ -1163,18 +1159,23 @@
             pltpu.VMEM((3, own_rows, width), bf16),
             pltpu.VMEM((2 * own_rows, width), bf16),
             pltpu.VMEM((rows + RIM, width), bf16),
+            pltpu.VMEM((rows, ff), f32),
             pltpu.VMEM((rows, ff), bf16),
             pltpu.VMEM(res.shape, bf16),
             pltpu.VMEM(rv.shape, bf16),
             pltpu.VMEM(mm.shape, bf16),
             dma((3,)),
             dma((3,)),
-            dma((units, 2, n_sp)),
-            dma((units, 2, planes // 2)),
-            dma((units, 2)),
-            dma((units, 2)),
             dma((units, planes)),
-            dma((units, n_sp)),
+            dma((CUTS[0] + CUTS[1],)),
+            dma((planes,)),
+            dma((2,)),
+            dma((n_sp,)),
+            dma((planes // 2,)),
+            dma,
+            dma,
+            dma,
+            dma((2,)),
             dma((3,)),
             dma((3,)),
             dma((2,)),
@@ -1190,9 +1191,9 @@
             dma((2, 2)),
             dma((4,)),
             dma,
-            dma((3, n_sp)),
-            dma((3, n_sp)),
-            dma((n_sp,)),
+            dma,
+            dma((3,)),
+            dma,
             dma((n_sp,)),
         ],
         compiler_params=pltpu.CompilerParams(
@@ -1215,7 +1216,8 @@
             and n_sp % (2 * FAN) == 0
             and n_sp > 2 * FAN
             and n_tp == 4
-            and args[18].shape[0] % 64 == 0
+            and args[18].shape[0] % 128 == 0
+            and args[18].shape[::-1] == args[16].shape
             and rows % (BLOCK * n_tp) == 0
         )
         if fits:

time: 140 us -> 135 us (0.964)
  Pallas kernels: 138 us -> 133 us
    pallas_call x1, Pallas kernels: 138 us -> 133 us  [fused_shards(): pl.pallas_call(functools.partial(layer_kernel, n_sp, n_tp), out_shape=jax...]
where the time goes in v3:
time: 135 us
  Pallas kernels  133 us (99%)
  local copies, waits for them, and re-layouts  1.88 us (1%)
    pallas_call x1, Pallas kernels, fused_shards(): pl.pallas_call(functools.partial(layer_kernel, n_sp, n_tp), out_shape=jax...  133 us

profile of v3, /device:TPU:19, one launch (start us, length us, event | category | flops | bytes accessed | tf_op | source)
XLA Modules:
  0.0 135.2 jit_solution(16036138075305883041)
XLA Ops:
  0.0 133.3 %shard_map.208 = bf16[128,2048]{1,0:T(8,128)(2,1)} custom-call(bf16[128,2048]{1,0:T(8,128)(2,1)} %res_hbm.1, bf16[512,512]{1,0:T(8,128)(2,1)} %rv_hbm.1, bf16[512,512]{1,0:T(8,128)(2,1)} %xf_ref.1, bf16[512,128]{1,0:T(8,128)(2,1)} %bf_ref.1, bf16[512,128]{1,0:T(8,128)(2,1)} %cf_ref.1, f32[8,512]{1,0:T(8,128)} %bitcast.8, f32[1,8]{1,0:T(1,128)} %bitcast.13, ...), custom_call_target="tpu_custom_call" | custom-call | tf_op jit(solution)/shard_map/pallas_call | solution.py:1124
  133.3 1.9 %copy.24 = bf16[128,2048]{1,0:T(8,128)(2,1)} copy(bf16[128,2048]{1,0:T(8,128)(2,1)} %shard_map.208) | data formatting | bytes 1048576

commit v4 on v3

--- a/solution.py
+++ b/solution.py
@@ -913,9 +913,10 @@
     relay_s(1)
     run_cols(up_cols, 0, full // 2)
     relay_s(2)
-    run_cols(up_cols, full // 2, full)
+    run_cols(up_cols, full // 2, full - 1)
+    send_z(both(shrink), lambda to: jnp.logical_and(far_outer(to), to > z))
+    run_cols(up_cols, full - 1, full)
     rest_cols(up_cols)
-    send_z(both(shrink), lambda to: jnp.logical_and(far_outer(to), to > z))
 
     def down(who):
         at = pl.ds(pl.multiple_of(who * cols, cols), cols)

time: 135 us -> 144 us (1.067)
  Pallas kernels: 133 us -> 142 us
    pallas_call x1, Pallas kernels: 133 us -> 142 us  [fused_shards(): pl.pallas_call(functools.partial(layer_kernel, n_sp, n_tp), out_shape=jax...]
where the time goes in v4:
time: 144 us
  Pallas kernels  142 us (99%)
  local copies, waits for them, and re-layouts  1.88 us (1%)
    pallas_call x1, Pallas kernels, fused_shards(): pl.pallas_call(functools.partial(layer_kernel, n_sp, n_tp), out_shape=jax...  142 us

profile of v4, /device:TPU:19, one launch (start us, length us, event | category | flops | bytes accessed | tf_op | source)
XLA Modules:
  0.0 144.2 jit_solution(12937220963441359057)
XLA Ops:
  0.0 142.3 %shard_map.208 = bf16[128,2048]{1,0:T(8,128)(2,1)} custom-call(bf16[128,2048]{1,0:T(8,128)(2,1)} %res_hbm.1, bf16[512,512]{1,0:T(8,128)(2,1)} %rv_hbm.1, bf16[512,512]{1,0:T(8,128)(2,1)} %xf_ref.1, bf16[512,128]{1,0:T(8,128)(2,1)} %bf_ref.1, bf16[512,128]{1,0:T(8,128)(2,1)} %cf_ref.1, f32[8,512]{1,0:T(8,128)} %bitcast.8, f32[1,8]{1,0:T(1,128)} %bitcast.13, ...), custom_call_target="tpu_custom_call" | custom-call | tf_op jit(solution)/shard_map/pallas_call | solution.py:1125
  142.3 1.9 %copy.24 = bf16[128,2048]{1,0:T(8,128)(2,1)} copy(bf16[128,2048]{1,0:T(8,128)(2,1)} %shard_map.208) | data formatting | bytes 1048576
